TPU v7x, 32 devices: a whole 2x2x4 slice. The times are simulated.
32 devices in a mesh: fs: 8 (over z, x), tp: 4 (over y, core).
Axes of the slice: x: 2, y: 2, z: 4, core: 2. Of those that a mesh axis runs over, the one named last changes fastest.
Arguments:
- tokens: bfloat16 [320, 4096], P('fs'), may hold values from -6 to 6
- routes: int32 [320, 2], P('fs'), may hold values from 0 to 3, all different within a row; in each aligned block of 40 rows (0 to 39, 40 to 79, ...) at most 30 rows name the same one
- route_logits: float32 [320, 2], P('fs'), may hold values from -6 to 6
- norm_gain: float32 [4096], P('fs'), may hold values from 0.1 to 1.9
- gate_weight: float32 [4, 4096, 8192], P(None, 'fs', 'tp'), may hold values from -0.09375 to 0.09375
- up_weight: float32 [4, 4096, 8192], P(None, 'fs', 'tp'), may hold values from -0.09375 to 0.09375
- down_weight: float32 [4, 4096, 8192], P(None, 'fs', 'tp'), may hold values from -0.0625 to 0.0625
Outputs:
- mixed: bfloat16 [320, 4096], P('fs', 'tp')
- gate_sampler: bfloat16 [4, 4096, 8192], P('tp', None, 'fs')
- up_sampler: bfloat16 [4, 4096, 8192], P('tp', None, 'fs')
- down_sampler: bfloat16 [4, 4096, 8192], P('tp', None, 'fs')
Inputs may be any that keep to these rules, and one draw needn't show every extreme that they name: `routes`: the 2 experts of a token differ. Within the tokens of one index of fs (aligned blocks of 40 rows) no expert is named by more than 30 tokens.
All inputs are finite; a program needn't handle non-finite values.
Results may differ from a plain program's by a relative error of at most 0.01.
Values may be sent and summed in bfloat16 or wider, within the bound.
No kernel may reach another device: no remote copies, remote signals or barrier semaphores. Data moves between devices by JAX's collectives and lax.ppermute only.
A program may use at most 192 MiB of HBM per device.

v0:
```python
import functools

import jax
import jax.numpy as jnp
from jax import lax
from jax.experimental import pallas as pl
from jax.experimental.pallas import tpu as pltpu
from jax.sharding import PartitionSpec as P


HBM = pltpu.MemorySpace.HBM
VMEM = pltpu.MemorySpace.VMEM
SMEM = pltpu.MemorySpace.SMEM


def swap(value, axis, k):
    count = lax.axis_size(axis)
    return lax.ppermute(value, axis, [(i, i ^ k) for i in range(count)])


def partner_orders(count, spread):
    near = [spread] + [k for k in range(1, count // 2) if k != spread]
    far = [k ^ 1 for k in range(count // 2, count)]
    half = len(far) // 2
    order = near[:1] + far[:half] + near[1:] + far[half:]
    first_order = far[:half][::-1] + near[1:] + near[:1] + far[half:]
    return near, far, first_order, order


def make_piece(weight, gain, dest, spread, columns, start, rows):
    spot = (lax.div(dest, spread), start, lax.rem(dest, spread) * columns)
    piece = lax.dynamic_slice(weight, spot, (1, rows, columns))[0]
    if gain is not None:
        piece = piece * gain[start : start + rows, None]
    return piece.astype(jnp.bfloat16)


def act_kernel(count, per_tp, keys, hidden, *refs):
    me_ref, x_ref = refs[:2]
    pieces = refs[2 : 2 + count]
    refs = refs[2 + count :]
    if hidden:
        gate_ref, out_ref, act_ref, held, acc, load_sem, store_sem = refs
    else:
        out_ref, act_ref, held, acc, load_sem, store_sem = refs
    rows = pieces[0].shape[0]
    loads = [
        pltpu.make_async_copy(pieces[j], held.at[j], load_sem.at[j]) for j in range(count)
    ]
    for load in loads:
        load.start()
    stores = []
    for j in range(count):
        slot = me_ref[0] ^ keys[j]
        loads[j].wait()
        store = pltpu.make_async_copy(
            held.at[j], out_ref.at[pl.ds(pl.multiple_of(slot * rows, rows), rows)], store_sem.at[j]
        )
        store.start()
        stores.append(store)
        which = (slot // per_tp ^ me_ref[1]) * per_tp + slot % per_tp
        part = jnp.dot(x_ref[which], held[j], preferred_element_type=jnp.float32)
        if j == 0:
            acc[...] = part
        else:
            acc[...] += part
    if hidden:
        gate = gate_ref[...]
        act_ref[...] = (gate / (1.0 + jnp.exp(-gate)) * acc[...]).astype(jnp.bfloat16)
    else:
        act_ref[...] = acc[...]
    for store in stores:
        store.wait()


def activate(me, x, pieces, keys, per_tp, gate=None):
    count = len(pieces)
    rows, columns = pieces[0].shape
    tokens = x.shape[1]
    args = [me, x, *pieces]
    in_specs = [pl.BlockSpec(memory_space=SMEM), pl.BlockSpec(memory_space=VMEM)]
    in_specs += [pl.BlockSpec(memory_space=HBM)] * count
    if gate is not None:
        args.append(gate)
        in_specs.append(pl.BlockSpec(memory_space=VMEM))
    act_type = jnp.float32 if gate is None else jnp.bfloat16
    return pl.pallas_call(
        functools.partial(act_kernel, count, per_tp, keys, gate is not None),
        in_specs=in_specs,
        out_specs=[pl.BlockSpec(memory_space=HBM), pl.BlockSpec(memory_space=VMEM)],
        out_shape=[
            jax.ShapeDtypeStruct((count * rows, columns), jnp.bfloat16),
            jax.ShapeDtypeStruct((tokens, columns), act_type),
        ],
        scratch_shapes=[
            pltpu.VMEM((count, rows, columns), jnp.bfloat16),
            pltpu.VMEM((tokens, columns), jnp.float32),
            pltpu.SemaphoreType.DMA((count,)),
            pltpu.SemaphoreType.DMA((count,)),
        ],
    )(*args)


def down_kernel(keys, offsets, rows, width, start, aliased, *refs):
    me_ref, hidden_ref, weight_ref = refs[:3]
    count = len(keys)
    pieces = refs[3 : 3 + count]
    refs = refs[3 + count + aliased :]
    out_ref, blocks = refs[0], refs[1:-3]
    held, load_sem, place_sem = refs[-3:]
    loads, places = [], []
    for j in range(count):
        slot = me_ref[0] ^ keys[j]
        spot = held.at[pl.ds(pl.multiple_of(slot * rows, rows), rows)]
        first = pl.multiple_of(slot * width + start, 16)
        piece = pieces[j].at[pl.ds(offsets[j], rows)]
        loads.append(pltpu.make_async_copy(piece, spot, load_sem.at[j]))
        places.append(
            pltpu.make_async_copy(spot, out_ref.at[pl.ds(first, rows)], place_sem.at[j])
        )
    for load in loads:
        load.start()
    for load, place in zip(loads, places):
        load.wait()
        place.start()
    span = held.shape[0] // len(blocks)
    for rel, block_ref in enumerate(blocks):
        block = me_ref[1] ^ rel
        part = lax.dot_general(
            hidden_ref[...],
            held[pl.ds(pl.multiple_of(block * span, span), span)],
            (((1,), (1,)), ((), ())),
            preferred_element_type=jnp.float32,
        )
        block_ref[...] = (part * weight_ref[...]).astype(jnp.bfloat16)
    for place in places:
        place.wait()


def down_partial(me, hidden, weight, pieces, keys, parts, width, start, rows, out):
    count = len(pieces)
    columns = pieces[0].shape[1]
    offsets = [start if piece.shape[0] == width else 0 for piece in pieces]
    tokens = hidden.shape[0]
    block = jax.ShapeDtypeStruct((tokens, count * rows // parts), jnp.bfloat16)
    args = [me, hidden, weight, *pieces]
    in_specs = [pl.BlockSpec(memory_space=SMEM)] + [pl.BlockSpec(memory_space=VMEM)] * 2
    in_specs += [pl.BlockSpec(memory_space=HBM)] * count
    aliases = {}
    if out is not None:
        aliases = {len(args): 0}
        args.append(out)
        in_specs.append(pl.BlockSpec(memory_space=HBM))
    return pl.pallas_call(
        functools.partial(down_kernel, keys, offsets, rows, width, start, len(aliases)),
        in_specs=in_specs,
        out_specs=[pl.BlockSpec(memory_space=HBM)] + [pl.BlockSpec(memory_space=VMEM)] * parts,
        out_shape=[jax.ShapeDtypeStruct((count * width, columns), jnp.bfloat16)] + [block] * parts,
        scratch_shapes=[
            pltpu.VMEM((count * rows, columns), jnp.bfloat16),
            pltpu.SemaphoreType.DMA((count,)),
            pltpu.SemaphoreType.DMA((count,)),
        ],
        input_output_aliases=aliases,
    )(*args)


def in_order(blocks, keys, me):
    stacked = jnp.stack(blocks)
    index = jnp.bitwise_xor(jnp.arange(len(keys)), me)
    where = jnp.argsort(jnp.array(keys))
    return stacked[jnp.take(where, index)]


def make_packet(tokens, routes, route_logits, experts):
    tok_float = tokens.astype(jnp.float32)
    normed = (
        tok_float * lax.rsqrt(jnp.mean(tok_float * tok_float, axis=1, keepdims=True) + 1e-05)
    ).astype(jnp.bfloat16)
    part_width = tokens.shape[1] // lax.axis_size("tp")
    own_cols = lax.dynamic_slice_in_dim(normed, lax.axis_index("tp") * part_width, part_width, 1)
    shares = jax.nn.sigmoid(route_logits - route_logits[:, ::-1])
    expert_ids = lax.broadcasted_iota(jnp.int32, (1, 1, experts), 2)
    weights = jnp.sum(jnp.where(routes[:, :, None] == expert_ids, shares[:, :, None], 0.0), axis=1)
    terms, rest = [], weights
    for _ in range(3):
        term = lax.reduce_precision(rest, 8, 7)
        terms.append(term.astype(jnp.bfloat16))
        rest = rest - term
    extra = jnp.concatenate(terms, axis=1)
    extra = jnp.pad(extra, ((0, 0), (0, -extra.shape[1] % 128)))
    return jnp.concatenate([own_cols, extra], axis=1)


def per_device(tokens, routes, route_logits, norm_gain, gate_weight, up_weight, down_weight):
    experts, width, _ = gate_weight.shape
    fs_count, tp_count = lax.axis_size("fs"), lax.axis_size("tp")
    fs_me, tp_me = lax.axis_index("fs"), lax.axis_index("tp")
    spread = fs_count // experts
    per_tp = fs_count // tp_count
    columns = gate_weight.shape[2] // spread
    own_rows, model = tokens.shape
    part_width = model // tp_count
    me = jnp.stack([fs_me, tp_me]).astype(jnp.int32)
    near, far, first_order, order = partner_orders(fs_count, spread)
    keys = [0] + near + far
    cuts = [0, width // 2, width * 3 // 4, width]
    spans = [(start, end - start) for start, end in zip(cuts, cuts[1:])]

    def fold(weight, gain, k, start=0, rows=width):
        return make_piece(weight, gain, fs_me ^ k, spread, columns, start, rows)

    def send(pieces):
        arrived = {}
        for k, piece in pieces.items():
            arrived[k] = swap(piece, "fs", k)
        return arrived

    first = fold(gate_weight, norm_gain, first_order[0])
    tokens, routes, route_logits, first = lax.optimization_barrier(
        (tokens, routes, route_logits, first)
    )
    packet = make_packet(tokens, routes, route_logits, experts)
    packet, gate_weight, first = lax.optimization_barrier((packet, gate_weight, first))
    groups = list(range(spread, fs_count, spread))
    held = [packet] + [swap(packet, "fs", k) for k in groups]
    gate_folds = {k: fold(gate_weight, norm_gain, k) for k in first_order[1:]}
    gate_folds, up_weight = lax.optimization_barrier((gate_folds, up_weight))
    gate_sent = send({first_order[0]: first, **gate_folds})
    up_folds = {k: fold(up_weight, norm_gain, k) for k in order}
    up_folds, down_weight = lax.optimization_barrier((up_folds, down_weight))
    up_sent = send(up_folds)
    down_folds = {k: fold(down_weight, None, k) for k in near}
    down_near = send(down_folds)
    down_far = [{k: fold(down_weight, None, k, *span) for k in far} for span in spans]
    down_sent = [send(folds) for folds in down_far]
    down_far, gate_weight, up_weight, down_weight = lax.optimization_barrier(
        (down_far, gate_weight, up_weight, down_weight)
    )
    gate_pieces = [fold(gate_weight, norm_gain, 0)] + [gate_sent[k] for k in keys[1:]]
    up_pieces = [fold(up_weight, norm_gain, 0)] + [up_sent[k] for k in keys[1:]]
    down_pieces = [
        [fold(down_weight, None, 0)] + [{**down_near, **sent}[k] for k in keys[1:]]
        for sent in down_sent
    ]

    held = in_order(held, list(range(experts)), lax.div(fs_me, spread))
    held = [held] + [swap(held, "fs", k) for k in range(1, spread)]
    held = in_order(held, list(range(spread)), lax.rem(fs_me, spread))
    gathered = jnp.swapaxes(held, 0, 1).reshape(fs_count * own_rows, packet.shape[1])
    block = gathered[:, :part_width]
    term_cols = gathered[:, part_width : part_width + 3 * experts].astype(jnp.float32)
    row_weights = jnp.sum(term_cols.reshape(-1, 3, experts), axis=1)
    mine = lax.broadcasted_iota(jnp.int32, (1, experts), 1) == lax.div(fs_me, spread)
    row_weight = jnp.sum(jnp.where(mine, row_weights, 0.0), axis=1, keepdims=True)
    blocks = jnp.stack([block] + [swap(block, "tp", k) for k in range(1, tp_count)])
    x = blocks.reshape(tp_count, -1, per_tp, width)
    x = jnp.transpose(x, (0, 2, 1, 3)).reshape(fs_count, -1, width)

    gate_out, gate_act = activate(me, x, gate_pieces, keys, per_tp)
    up_out, hidden = activate(me, x, up_pieces, keys, per_tp, gate_act)

    down_out = None
    totals = []
    for span, pieces in zip(spans, down_pieces):
        down_out, *parts = down_partial(
            me, hidden, row_weight, pieces, keys, tp_count, width, *span, down_out
        )
        total = parts[0].astype(jnp.float32)
        for k in range(1, tp_count):
            total = total + swap(parts[k], "tp", k).astype(jnp.float32)
        totals.append(total.astype(jnp.bfloat16).reshape(fs_count, own_rows, -1))
    done = []
    for group in [totals[:-1], totals[-1:]]:
        away = jnp.concatenate(group, axis=2)
        back = lax.all_to_all(away, "fs", split_axis=0, concat_axis=0, tiled=True)
        ends = [part.shape[2] for part in group]
        ends = [sum(ends[: i + 1]) for i in range(len(ends) - 1)]
        back = jnp.sum(back.astype(jnp.float32), axis=0).astype(jnp.bfloat16)
        done += jnp.split(back, ends, axis=1)
    mixed = jnp.concatenate([part.reshape(own_rows, per_tp, -1) for part in done], axis=2)
    return mixed.reshape(own_rows, part_width), gate_out[None], up_out[None], down_out[None]


def solution(mesh):
    in_specs = (
        P("fs", None),
        P("fs", None),
        P("fs", None),
        P("fs"),
        P(None, "fs", "tp"),
        P(None, "fs", "tp"),
        P(None, "fs", "tp"),
    )
    out_specs = (P("fs", "tp"), P("tp", None, "fs"), P("tp", None, "fs"), P("tp", None, "fs"))

    return jax.shard_map(
        per_device, mesh=mesh, in_specs=in_specs, out_specs=out_specs, check_vma=False
    )
```

profile of v0, /device:TPU:0, one launch (start us, length us, event | category | flops | bytes accessed | tf_op | source)
XLA Modules:
  0.0 666.9 jit_solution(9566284548473041782)
XLA Ops:
  0.7 1.8 fusion.15
  3.1 5.1 collective-permute-start.2
  8.9 8.7 %fusion.9 = (bf16[512,1024]{1,0:T(8,128)(2,1)}, bf16[512,1024]{1,0:T(8,128)(2,1)}, bf16[512,1024]{1,0:T(8,128)(2,1)}, bf16[512,1024]{1,0:T(8,128)(2,1)}, bf16[51...) fusion(f32[4,512,2048]{2,1,0:T(8,128)} %param.13, s32[]{:T(128)S(6)} %select_n.209, s32[]{:T(128)S(6)} %select_n.210, ...), kind=kLoop, calls=%fused_computation.25 | loop fusion | flops 6291456 | bytes 18876464 | tf_op jit(solution)/shard_map/convert_element_type | solution.py:35
  17.6 9.5 %fusion.2 = (bf16[512,1024]{1,0:T(8,128)(2,1)}, bf16[512,1024]{1,0:T(8,128)(2,1)}, bf16[512,1024]{1,0:T(8,128)(2,1)}, bf16[512,1024]{1,0:T(8,128)(2,1)S(1)}, bf1...) fusion(f32[4,512,2048]{2,1,0:T(8,128)} %param.14, s32[]{:T(128)S(6)} %select_n.209, ...), kind=kLoop, calls=%fused_computation.11 | loop fusion | flops 7340032 | bytes 22022200 | tf_op jit(solution)/shard_map/convert_element_type | solution.py:35
  27.1 3.6 fusion.23
  30.7 4.7 collective-permute-start.26
  38.2 3.5 fusion.31
  41.7 1.0 collective-permute-start.33
  42.7 3.6 collective-permute-start.34
  46.3 7.5 %collective-permute-done.33.refs_9_ = bf16[128,1024]{1,0:T(8,128)(2,1)S(1)} collective-permute-done((bf16[128,1024]{1,0:T(8,128)(2,1)S(1)}, bf16[128,1024]{1,0:T(8,128)(2,1)S(1)}, u32[]{:S(2)}, u32[]{:S(2)}) %collective-permute-start.33) | collective-permute-done | bytes 262176 | tf_op jit(solution)/shard_map/ppermute | solution.py:18
  53.8 4.1 collective-permute-start.27
  57.9 1.7 collective-permute-done.34.refs_10_
  59.6 39.9 %collective-permute-start.24 = (bf16[256,1024]{1,0:T(8,128)(2,1)S(1)}, bf16[256,1024]{1,0:T(8,128)(2,1)S(1)}, u32[]{:S(2)}, u32[]{:S(2)}) collective-permute-start(bf16[256,1024]{1,0:T(8,128)(2,1)S(1)} %copy-done.17), channel_id=1, source_target_pairs={{0,20},{4,16},{8,28},{12,24},{16,4},{20,0},{24,12},{28,8},{1,21},{... | collective-permute-start | bytes 1572872 | tf_op jit(solution)/shard_map/ppermute | solution.py:18
  99.5 14.8 %collective-permute-done.31.refs_7_ = bf16[128,1024]{1,0:T(8,128)(2,1)S(1)} collective-permute-done((bf16[128,1024]{1,0:T(8,128)(2,1)S(1)}, bf16[128,1024]{1,0:T(8,128)(2,1)S(1)}, u32[]{:S(2)}, u32[]{:S(2)}) %collective-permute-start.31) | collective-permute-done | bytes 262176 | tf_op jit(solution)/shard_map/ppermute | solution.py:18
  114.9 2.3 collective-permute-start.18
  117.2 1.3 collective-permute-start.14
  118.5 32.8 %collective-permute-start.15 = (bf16[512,1024]{1,0:T(8,128)(2,1)}, bf16[512,1024]{1,0:T(8,128)(2,1)}, u32[]{:S(2)}, u32[]{:S(2)}) collective-permute-start(bf16[512,1024]{1,0:T(8,128)(2,1)} %get-tuple-element.70), channel_id=1, source_target_pairs={{0,4},{4,0},{8,12},{12,8},{16,20},{20,16},{24,28},{28,24},{1,5},{5... | collective-permute-start | bytes 3145736 | tf_op jit(solution)/shard_map/ppermute | solution.py:18
  151.4 19.0 %collective-permute-done.24.refs_7_ = bf16[256,1024]{1,0:T(8,128)(2,1)S(1)} collective-permute-done((bf16[256,1024]{1,0:T(8,128)(2,1)S(1)}, bf16[256,1024]{1,0:T(8,128)(2,1)S(1)}, u32[]{:S(2)}, u32[]{:S(2)}) %collective-permute-start.24) | collective-permute-done | bytes 524320 | tf_op jit(solution)/shard_map/ppermute | solution.py:18
  170.6 11.2 %collective-permute-done.25.refs_8_ = bf16[256,1024]{1,0:T(8,128)(2,1)S(1)} collective-permute-done((bf16[256,1024]{1,0:T(8,128)(2,1)S(1)}, bf16[256,1024]{1,0:T(8,128)(2,1)S(1)}, u32[]{:S(2)}, u32[]{:S(2)}) %collective-permute-start.25) | collective-permute-done | bytes 524320 | tf_op jit(solution)/shard_map/ppermute | solution.py:18
  181.8 44.9 %collective-permute-done.18.refs_7_ = bf16[512,1024]{1,0:T(8,128)(2,1)S(1)} collective-permute-done((bf16[512,1024]{1,0:T(8,128)(2,1)S(1)}, bf16[512,1024]{1,0:T(8,128)(2,1)S(1)}, u32[]{:S(2)}, u32[]{:S(2)}) %collective-permute-start.18) | collective-permute-done | bytes 1048608 | tf_op jit(solution)/shard_map/ppermute | solution.py:18
  226.7 3.0 collective-permute-start.19
  229.7 1.0 copy-done.7
  230.7 0.9 collective-permute-start.20
  232.3 1.4 collective-permute-start.8
  233.8 60.4 %collective-permute-done.17.refs_6_ = bf16[512,1024]{1,0:T(8,128)(2,1)} collective-permute-done((bf16[512,1024]{1,0:T(8,128)(2,1)}, bf16[512,1024]{1,0:T(8,128)(2,1)}, u32[]{:S(2)}, u32[]{:S(2)}) %collective-permute-start.17) | collective-permute-done | bytes 1048608 | tf_op jit(solution)/shard_map/ppermute | solution.py:18
  295.1 43.9 %collective-permute-start.10 = (bf16[512,1024]{1,0:T(8,128)(2,1)}, bf16[512,1024]{1,0:T(8,128)(2,1)}, u32[]{:S(2)}, u32[]{:S(2)}) collective-permute-start(bf16[512,1024]{1,0:T(8,128)(2,1)} %get-tuple-element.64), channel_id=1, source_target_pairs={{0,20},{4,16},{8,28},{12,24},{16,4},{20,0},{24,12},{28,8},{1,21},{... | collective-permute-start | bytes 3145736 | tf_op jit(solution)/shard_map/ppermute | solution.py:18
  339.0 43.1 %collective-permute-start.11 = (bf16[512,1024]{1,0:T(8,128)(2,1)S(1)}, bf16[512,1024]{1,0:T(8,128)(2,1)}, u32[]{:S(2)}, u32[]{:S(2)}) collective-permute-start(bf16[512,1024]{1,0:T(8,128)(2,1)S(1)} %get-tuple-element.65), channel_id=1, source_target_pairs={{0,16},{4,20},{8,24},{12,28},{16,0},{20,4},{24,8},{28,12},{1,17},{... | collective-permute-start | bytes 3145736 | tf_op jit(solution)/shard_map/ppermute | solution.py:18
  382.1 1.1 pad_maximum_fusion.2
  384.8 1.0 slice_bitcast_fusion
  385.8 1.5 collective-permute-start.5
  388.0 4.7 fusion.19
  392.6 30.9 %collective-permute-done.10.refs_6_ = bf16[512,1024]{1,0:T(8,128)(2,1)} collective-permute-done((bf16[512,1024]{1,0:T(8,128)(2,1)}, bf16[512,1024]{1,0:T(8,128)(2,1)}, u32[]{:S(2)}, u32[]{:S(2)}) %collective-permute-start.10) | collective-permute-done | bytes 1048608 | tf_op jit(solution)/shard_map/ppermute | solution.py:18
  423.6 5.3 collective-permute-start.12
  428.9 40.9 %collective-permute-done.11.refs_7_ = bf16[512,1024]{1,0:T(8,128)(2,1)} collective-permute-done((bf16[512,1024]{1,0:T(8,128)(2,1)S(1)}, bf16[512,1024]{1,0:T(8,128)(2,1)}, u32[]{:S(2)}, u32[]{:S(2)}) %collective-permute-start.11) | collective-permute-done | bytes 1048608 | tf_op jit(solution)/shard_map/ppermute | solution.py:18
  469.8 3.1 collective-permute-start.13
  474.9 3.3 collective-permute-start.21
  478.7 2.7 fusion.16.refs_3_
  481.4 3.8 fusion
  487.2 2.0 pad_maximum_fusion
  489.4 8.6 %collective-permute-done.13.refs_9_ = bf16[512,1024]{1,0:T(8,128)(2,1)} collective-permute-done((bf16[512,1024]{1,0:T(8,128)(2,1)}, bf16[512,1024]{1,0:T(8,128)(2,1)}, u32[]{:S(2)}, u32[]{:S(2)}) %collective-permute-start.13) | collective-permute-done | bytes 1048608 | tf_op jit(solution)/shard_map/ppermute | solution.py:18
  497.9 3.1 collective-permute-start.41
  501.1 31.7 %collective-permute-done.23.refs_6_ = bf16[512,1024]{1,0:T(8,128)(2,1)S(1)} collective-permute-done((bf16[512,1024]{1,0:T(8,128)(2,1)}, bf16[512,1024]{1,0:T(8,128)(2,1)S(1)}, u32[]{:S(2)}, u32[]{:S(2)}) %collective-permute-start.23) | collective-permute-done | bytes 1048608 | tf_op jit(solution)/shard_map/ppermute | solution.py:18
  532.8 20.6 %collective-permute-start.38 = (bf16[128,1024]{1,0:T(8,128)(2,1)}, bf16[128,1024]{1,0:T(8,128)(2,1)}, u32[]{:S(2)}, u32[]{:S(2)}) collective-permute-start(bf16[128,1024]{1,0:T(8,128)(2,1)} %get-tuple-element.114), channel_id=1, source_target_pairs={{0,20},{4,16},{8,28},{12,24},{16,4},{20,0},{24,12},{28,8},{1,21},{... | collective-permute-start | bytes 786440 | tf_op jit(solution)/shard_map/ppermute | solution.py:18
  553.4 1.5 collective-permute-start.39
  555.3 3.2 collective-permute-start.32
  558.7 1.7 pad_maximum_fusion.1
  560.4 9.5 %shard_map.120 = (bf16[4096,1024]{1,0:T(8,128)(2,1)}, f32[320,1024]{1,0:T(8,128)}) custom-call(s32[2]{0:T(128)} %pad_add_fusion.refs_0_, bf16[8,320,512]{2,1,0:T(8,128)(2,1)} %bitcast.139, bf16[512,1024]{1,0:T(8,128)(2,1)} %get-tuple-element.128.refs_2_, bf16[512,1024]{1,0:T(8,128)(2,1)} %copy-done.7, bf16[512,1024]{1,0:T(8,128)(2,1)} %collective-permute-done.15.refs_4_, ...), custom_call_target="tpu_custom_call" | custom-call | tf_op jit(solution)/shard_map/pallas_call | solution.py:87
  569.9 9.4 %shard_map.121 = (bf16[4096,1024]{1,0:T(8,128)(2,1)}, bf16[320,1024]{1,0:T(8,128)(2,1)}) custom-call(s32[2]{0:T(128)} %pad_add_fusion.refs_0_, bf16[8,320,512]{2,1,0:T(8,128)(2,1)} %bitcast.140, bf16[512,1024]{1,0:T(8,128)(2,1)} %get-tuple-element.129.refs_2_, bf16[512,1024]{1,0:T(8,128)(2,1)} %collective-permute-done.7.refs_3_, ...), custom_call_target="tpu_custom_call" | custom-call | tf_op jit(solution)/shard_map/pallas_call | solution.py:87
  579.3 6.6 shard_map.122
  585.9 19.9 %collective-permute-done.32.refs_8_ = bf16[128,1024]{1,0:T(8,128)(2,1)} collective-permute-done((bf16[128,1024]{1,0:T(8,128)(2,1)}, bf16[128,1024]{1,0:T(8,128)(2,1)}, u32[]{:S(2)}, u32[]{:S(2)}) %collective-permute-start.32) | collective-permute-done | bytes 262176 | tf_op jit(solution)/shard_map/ppermute | solution.py:18
  605.9 4.5 shard_map.123
  611.2 4.6 shard_map.124
  616.4 1.5 collective-permute-start.43
  618.5 1.5 collective-permute-start.29
  620.1 3.6 collective-permute-done.43
  623.7 1.5 collective-permute-start.36
  625.2 1.1 collective-permute-done.44
  626.3 1.8 collective-permute-start.37
  628.1 1.7 add_convert_fusion.1
  629.8 3.4 all-to-all-start.1
  633.2 11.6 %collective-permute-done.36 = bf16[320,256]{1,0:T(8,128)(2,1)S(1)} collective-permute-done((bf16[320,256]{1,0:T(8,128)(2,1)}, bf16[320,256]{1,0:T(8,128)(2,1)S(1)}, u32[]{:S(2)}, u32[]{:S(2)}) %collective-permute-start.36) | collective-permute-done | bytes 163872 | tf_op jit(solution)/shard_map/ppermute | solution.py:18
  644.7 1.8 collective-permute-done.37
  647.7 3.5 all-to-all-start
  651.2 14.8 %all-to-all-done = bf16[8,40,768]{2,1,0:T(8,128)(2,1)S(1)} async-done(((bf16[8,40,768]{2,1,0:T(8,128)(2,1)}), bf16[8,40,768]{2,1,0:T(8,128)(2,1)S(1)}, u32[]{:S(2)}, u32[]{:S(2)}) %all-to-all-start) | async-done | bytes 491552 | tf_op jit(solution)/shard_map/all_to_all | solution.py:276
  (162 shorter events, 17.8 us)
Async XLA Ops:
  0.7 8.2 %copy-start.26 = (f32[512]{0:T(512)S(1)}, f32[512]{0:T(512)}, u32[]{:S(2)}) copy-start(f32[512]{0:T(512)} %param.12) | copy-start | bytes 6148
  3.1 33.7 %collective-permute-start.2 = (bf16[40,1152]{1,0:T(8,128)(2,1)S(1)}, bf16[40,1152]{1,0:T(8,128)(2,1)S(1)}, u32[]{:S(2)}, u32[]{:S(2)}) collective-permute-start(bf16[40,1152]{1,0:T(8,128)(2,1)S(1)} %fusion.34), channel_id=1, source_target_pairs={{0,24},{4,28},{8,16},{12,20},{16,8},{20,12},{24,0},{28,4},{1,25},{... | collective-permute-start | bytes 276488 | tf_op jit(solution)/shard_map/ppermute | solution.py:18
  8.3 28.6 %collective-permute-start.1 = (bf16[40,1152]{1,0:T(8,128)(2,1)S(1)}, bf16[40,1152]{1,0:T(8,128)(2,1)S(1)}, u32[]{:S(2)}, u32[]{:S(2)}) collective-permute-start(bf16[40,1152]{1,0:T(8,128)(2,1)S(1)} %fusion.34), channel_id=1, source_target_pairs={{0,16},{4,20},{8,24},{12,28},{16,0},{20,4},{24,8},{28,12},{1,17},{... | collective-permute-start | bytes 276488 | tf_op jit(solution)/shard_map/ppermute | solution.py:18
  8.3 28.6 %collective-permute-start = (bf16[40,1152]{1,0:T(8,128)(2,1)S(1)}, bf16[40,1152]{1,0:T(8,128)(2,1)S(1)}, u32[]{:S(2)}, u32[]{:S(2)}) collective-permute-start(bf16[40,1152]{1,0:T(8,128)(2,1)S(1)} %fusion.34), channel_id=1, source_target_pairs={{0,8},{4,12},{8,0},{12,4},{16,24},{20,28},{24,16},{28,20},{1,9},{5... | collective-permute-start | bytes 276488 | tf_op jit(solution)/shard_map/ppermute | solution.py:18
  30.7 86.5 %collective-permute-start.26 = (bf16[256,1024]{1,0:T(8,128)(2,1)}, bf16[256,1024]{1,0:T(8,128)(2,1)S(1)}, u32[]{:S(2)}, u32[]{:S(2)}) collective-permute-start(bf16[256,1024]{1,0:T(8,128)(2,1)} %get-tuple-element.120), channel_id=1, source_target_pairs={{0,28},{4,24},{8,20},{12,16},{16,12},{20,8},{24,4},{28,0},{1,29},{... | collective-permute-start | bytes 1572872 | tf_op jit(solution)/shard_map/ppermute | solution.py:18
  37.5 16.3 %copy-start.18 = (bf16[256,1024]{1,0:T(8,128)(2,1)S(1)}, bf16[256,1024]{1,0:T(8,128)(2,1)}, u32[]{:S(2)}) copy-start(bf16[256,1024]{1,0:T(8,128)(2,1)} %get-tuple-element.121) | copy-start | bytes 1572868
  37.5 22.0 %copy-start.17 = (bf16[256,1024]{1,0:T(8,128)(2,1)S(1)}, bf16[256,1024]{1,0:T(8,128)(2,1)}, u32[]{:S(2)}) copy-start(bf16[256,1024]{1,0:T(8,128)(2,1)} %get-tuple-element.122) | copy-start | bytes 1572868
  37.6 76.7 %copy-start.16 = (bf16[256,1024]{1,0:T(8,128)(2,1)S(1)}, bf16[256,1024]{1,0:T(8,128)(2,1)}, u32[]{:S(2)}) copy-start(bf16[256,1024]{1,0:T(8,128)(2,1)} %get-tuple-element.123) | copy-start | bytes 1572868
  37.6 79.7 %copy-start.5 = (bf16[512,1024]{1,0:T(8,128)(2,1)S(1)}, bf16[512,1024]{1,0:T(8,128)(2,1)}, u32[]{:S(2)}) copy-start(bf16[512,1024]{1,0:T(8,128)(2,1)} %get-tuple-element.69) | copy-start | bytes 3145732
  37.6 77.3 %collective-permute-start.3 = (bf16[4,40,1152]{2,1,0:T(8,128)(2,1)S(1)}, bf16[4,40,1152]{2,1,0:T(8,128)(2,1)S(1)}, u32[]{:S(2)}, u32[]{:S(2)}) collective-permute-start(bf16[4,40,1152]{2,1,0:T(8,128)(2,1)S(1)} %gather_fusion.1), channel_id=1, source_target_pairs={{0,4},{4,0},{8,12},{12,8},{16,20},{20,16},{24,28},{28,24},{1,5},{5... | collective-permute-start | bytes 1105928 | tf_op jit(solution)/shard_map/ppermute | solution.py:18
  41.7 12.1 %collective-permute-start.33 = (bf16[128,1024]{1,0:T(8,128)(2,1)S(1)}, bf16[128,1024]{1,0:T(8,128)(2,1)S(1)}, u32[]{:S(2)}, u32[]{:S(2)}) collective-permute-start(bf16[128,1024]{1,0:T(8,128)(2,1)S(1)} %get-tuple-element.116), channel_id=1, source_target_pairs={{0,28},{4,24},{8,20},{12,16},{16,12},{20,8},{24,4},{28,0},{1,29},{... | collective-permute-start | bytes 786440 | tf_op jit(solution)/shard_map/ppermute | solution.py:18
  42.7 16.9 %collective-permute-start.34 = (bf16[128,1024]{1,0:T(8,128)(2,1)S(1)}, bf16[128,1024]{1,0:T(8,128)(2,1)S(1)}, u32[]{:S(2)}, u32[]{:S(2)}) collective-permute-start(bf16[128,1024]{1,0:T(8,128)(2,1)S(1)} %get-tuple-element.117), channel_id=1, source_target_pairs={{0,24},{4,28},{8,16},{12,20},{16,8},{20,12},{24,0},{28,4},{1,25},{... | collective-permute-start | bytes 786440 | tf_op jit(solution)/shard_map/ppermute | solution.py:18
  46.3 67.9 %collective-permute-start.31 = (bf16[128,1024]{1,0:T(8,128)(2,1)S(1)}, bf16[128,1024]{1,0:T(8,128)(2,1)S(1)}, u32[]{:S(2)}, u32[]{:S(2)}) collective-permute-start(bf16[128,1024]{1,0:T(8,128)(2,1)S(1)} %get-tuple-element.118), channel_id=1, source_target_pairs={{0,20},{4,16},{8,28},{12,24},{16,4},{20,0},{24,12},{28,8},{1,21},{... | collective-permute-start | bytes 786440 | tf_op jit(solution)/shard_map/ppermute | solution.py:18
  53.8 60.4 %copy-start.21 = (bf16[128,1024]{1,0:T(8,128)(2,1)}, bf16[128,1024]{1,0:T(8,128)(2,1)S(1)}, u32[]{:S(2)}) copy-start(bf16[128,1024]{1,0:T(8,128)(2,1)S(1)} %collective-permute-done.33.refs_9_) | copy-start | bytes 786436
  53.8 64.7 %collective-permute-start.27 = (bf16[256,1024]{1,0:T(8,128)(2,1)S(1)}, bf16[256,1024]{1,0:T(8,128)(2,1)S(1)}, u32[]{:S(2)}, u32[]{:S(2)}) collective-permute-start(bf16[256,1024]{1,0:T(8,128)(2,1)S(1)} %copy-done.18), channel_id=1, source_target_pairs={{0,24},{4,28},{8,16},{12,20},{16,8},{20,12},{24,0},{28,4},{1,25},{... | collective-permute-start | bytes 1572872 | tf_op jit(solution)/shard_map/ppermute | solution.py:18
  59.6 54.7 %copy-start.22 = (bf16[128,1024]{1,0:T(8,128)(2,1)}, bf16[128,1024]{1,0:T(8,128)(2,1)S(1)}, u32[]{:S(2)}) copy-start(bf16[128,1024]{1,0:T(8,128)(2,1)S(1)} %collective-permute-done.34.refs_10_) | copy-start | bytes 786436
  59.6 110.8 %collective-permute-start.24 = (bf16[256,1024]{1,0:T(8,128)(2,1)S(1)}, bf16[256,1024]{1,0:T(8,128)(2,1)S(1)}, u32[]{:S(2)}, u32[]{:S(2)}) collective-permute-start(bf16[256,1024]{1,0:T(8,128)(2,1)S(1)} %copy-done.17), channel_id=1, source_target_pairs={{0,20},{4,16},{8,28},{12,24},{16,4},{20,0},{24,12},{28,8},{1,21},{... | collective-permute-start | bytes 1572872 | tf_op jit(solution)/shard_map/ppermute | solution.py:18
  114.2 67.6 %collective-permute-start.25 = (bf16[256,1024]{1,0:T(8,128)(2,1)S(1)}, bf16[256,1024]{1,0:T(8,128)(2,1)S(1)}, u32[]{:S(2)}, u32[]{:S(2)}) collective-permute-start(bf16[256,1024]{1,0:T(8,128)(2,1)S(1)} %copy-done.16), channel_id=1, source_target_pairs={{0,16},{4,20},{8,24},{12,28},{16,0},{20,4},{24,8},{28,12},{1,17},{... | collective-permute-start | bytes 1572872 | tf_op jit(solution)/shard_map/ppermute | solution.py:18
  114.9 66.9 %copy-start.19 = (bf16[4,40,1152]{2,1,0:T(8,128)(2,1)}, bf16[4,40,1152]{2,1,0:T(8,128)(2,1)S(1)}, u32[]{:S(2)}) copy-start(bf16[4,40,1152]{2,1,0:T(8,128)(2,1)S(1)} %collective-permute-done.3) | copy-start | bytes 1105924
  114.9 111.8 %collective-permute-start.18 = (bf16[512,1024]{1,0:T(8,128)(2,1)S(1)}, bf16[512,1024]{1,0:T(8,128)(2,1)S(1)}, u32[]{:S(2)}, u32[]{:S(2)}) collective-permute-start(bf16[512,1024]{1,0:T(8,128)(2,1)S(1)} %fusion.15), channel_id=1, source_target_pairs={{0,16},{4,20},{8,24},{12,28},{16,0},{20,4},{24,8},{28,12},{1,17},{... | collective-permute-start | bytes 3145736 | tf_op jit(solution)/shard_map/ppermute | solution.py:18
  117.2 275.4 %copy-start.12 = (bf16[256,1024]{1,0:T(8,128)(2,1)}, bf16[256,1024]{1,0:T(8,128)(2,1)S(1)}, u32[]{:S(2)}) copy-start(bf16[256,1024]{1,0:T(8,128)(2,1)S(1)} %collective-permute-done.26.refs_9_) | copy-start | bytes 1572868
  117.2 112.5 %collective-permute-start.14 = (bf16[512,1024]{1,0:T(8,128)(2,1)S(1)}, bf16[512,1024]{1,0:T(8,128)(2,1)S(1)}, u32[]{:S(2)}, u32[]{:S(2)}) collective-permute-start(bf16[512,1024]{1,0:T(8,128)(2,1)S(1)} %copy-done.5), channel_id=1, source_target_pairs={{0,8},{4,12},{8,0},{12,4},{16,24},{20,28},{24,16},{28,20},{1,9},{5... | collective-permute-start | bytes 3145736 | tf_op jit(solution)/shard_map/ppermute | solution.py:18
  118.5 111.2 %copy-start.13 = (bf16[256,1024]{1,0:T(8,128)(2,1)}, bf16[256,1024]{1,0:T(8,128)(2,1)S(1)}, u32[]{:S(2)}) copy-start(bf16[256,1024]{1,0:T(8,128)(2,1)S(1)} %collective-permute-done.27.refs_10_) | copy-start | bytes 1572868
  118.5 113.8 %collective-permute-start.15 = (bf16[512,1024]{1,0:T(8,128)(2,1)}, bf16[512,1024]{1,0:T(8,128)(2,1)}, u32[]{:S(2)}, u32[]{:S(2)}) collective-permute-start(bf16[512,1024]{1,0:T(8,128)(2,1)} %get-tuple-element.70), channel_id=1, source_target_pairs={{0,4},{4,0},{8,12},{12,8},{16,20},{20,16},{24,28},{28,24},{1,5},{5... | collective-permute-start | bytes 3145736 | tf_op jit(solution)/shard_map/ppermute | solution.py:18
  170.4 59.3 %copy-start.14 = (bf16[256,1024]{1,0:T(8,128)(2,1)}, bf16[256,1024]{1,0:T(8,128)(2,1)S(1)}, u32[]{:S(2)}) copy-start(bf16[256,1024]{1,0:T(8,128)(2,1)S(1)} %collective-permute-done.24.refs_7_) | copy-start | bytes 1572868
  170.4 61.9 %collective-permute-start.16 = (bf16[512,1024]{1,0:T(8,128)(2,1)}, bf16[512,1024]{1,0:T(8,128)(2,1)}, u32[]{:S(2)}, u32[]{:S(2)}) collective-permute-start(bf16[512,1024]{1,0:T(8,128)(2,1)} %get-tuple-element.71), channel_id=1, source_target_pairs={{0,12},{4,8},{8,4},{12,0},{16,28},{20,24},{24,20},{28,16},{1,13},{... | collective-permute-start | bytes 3145736 | tf_op jit(solution)/shard_map/ppermute | solution.py:18
  181.8 47.9 %copy-start.15 = (bf16[256,1024]{1,0:T(8,128)(2,1)}, bf16[256,1024]{1,0:T(8,128)(2,1)S(1)}, u32[]{:S(2)}) copy-start(bf16[256,1024]{1,0:T(8,128)(2,1)S(1)} %collective-permute-done.25.refs_8_) | copy-start | bytes 1572868
  181.8 112.4 %collective-permute-start.17 = (bf16[512,1024]{1,0:T(8,128)(2,1)}, bf16[512,1024]{1,0:T(8,128)(2,1)}, u32[]{:S(2)}, u32[]{:S(2)}) collective-permute-start(bf16[512,1024]{1,0:T(8,128)(2,1)} %get-tuple-element.72), channel_id=1, source_target_pairs={{0,20},{4,16},{8,28},{12,24},{16,4},{20,0},{24,12},{28,8},{1,21},{... | collective-permute-start | bytes 3145736 | tf_op jit(solution)/shard_map/ppermute | solution.py:18
  226.7 68.4 %collective-permute-start.19 = (bf16[512,1024]{1,0:T(8,128)(2,1)}, bf16[512,1024]{1,0:T(8,128)(2,1)S(1)}, u32[]{:S(2)}, u32[]{:S(2)}) collective-permute-start(bf16[512,1024]{1,0:T(8,128)(2,1)} %get-tuple-element.74), channel_id=1, source_target_pairs={{0,28},{4,24},{8,20},{12,16},{16,12},{20,8},{24,4},{28,0},{1,29},{... | collective-permute-start | bytes 3145736 | tf_op jit(solution)/shard_map/ppermute | solution.py:18
  230.7 108.3 %collective-permute-start.20 = (bf16[512,1024]{1,0:T(8,128)(2,1)}, bf16[512,1024]{1,0:T(8,128)(2,1)}, u32[]{:S(2)}, u32[]{:S(2)}) collective-permute-start(bf16[512,1024]{1,0:T(8,128)(2,1)} %get-tuple-element.75), channel_id=1, source_target_pairs={{0,24},{4,28},{8,16},{12,20},{16,8},{20,12},{24,0},{28,4},{1,25},{... | collective-permute-start | bytes 3145736 | tf_op jit(solution)/shard_map/ppermute | solution.py:18
  232.3 153.5 %collective-permute-start.7 = (bf16[512,1024]{1,0:T(8,128)(2,1)}, bf16[512,1024]{1,0:T(8,128)(2,1)}, u32[]{:S(2)}, u32[]{:S(2)}) collective-permute-start(bf16[512,1024]{1,0:T(8,128)(2,1)} %get-tuple-element.61), channel_id=1, source_target_pairs={{0,8},{4,12},{8,0},{12,4},{16,24},{20,28},{24,16},{28,20},{1,9},{5... | collective-permute-start | bytes 3145736 | tf_op jit(solution)/shard_map/ppermute | solution.py:18
  232.3 155.0 %collective-permute-start.8 = (bf16[512,1024]{1,0:T(8,128)(2,1)}, bf16[512,1024]{1,0:T(8,128)(2,1)}, u32[]{:S(2)}, u32[]{:S(2)}) collective-permute-start(bf16[512,1024]{1,0:T(8,128)(2,1)} %get-tuple-element.62), channel_id=1, source_target_pairs={{0,4},{4,0},{8,12},{12,8},{16,20},{20,16},{24,28},{28,24},{1,5},{5... | collective-permute-start | bytes 3145736 | tf_op jit(solution)/shard_map/ppermute | solution.py:18
  294.2 93.2 %collective-permute-start.9 = (bf16[512,1024]{1,0:T(8,128)(2,1)}, bf16[512,1024]{1,0:T(8,128)(2,1)}, u32[]{:S(2)}, u32[]{:S(2)}) collective-permute-start(bf16[512,1024]{1,0:T(8,128)(2,1)} %get-tuple-element.63), channel_id=1, source_target_pairs={{0,12},{4,8},{8,4},{12,0},{16,28},{20,24},{24,20},{28,16},{1,13},{... | collective-permute-start | bytes 3145736 | tf_op jit(solution)/shard_map/ppermute | solution.py:18
  295.1 87.1 %copy-start.8 = (bf16[512,1024]{1,0:T(8,128)(2,1)}, bf16[512,1024]{1,0:T(8,128)(2,1)S(1)}, u32[]{:S(2)}) copy-start(bf16[512,1024]{1,0:T(8,128)(2,1)S(1)} %collective-permute-done.19.refs_8_) | copy-start | bytes 3145732
  295.1 128.5 %collective-permute-start.10 = (bf16[512,1024]{1,0:T(8,128)(2,1)}, bf16[512,1024]{1,0:T(8,128)(2,1)}, u32[]{:S(2)}, u32[]{:S(2)}) collective-permute-start(bf16[512,1024]{1,0:T(8,128)(2,1)} %get-tuple-element.64), channel_id=1, source_target_pairs={{0,20},{4,16},{8,28},{12,24},{16,4},{20,0},{24,12},{28,8},{1,21},{... | collective-permute-start | bytes 3145736 | tf_op jit(solution)/shard_map/ppermute | solution.py:18
  339.0 130.8 %collective-permute-start.11 = (bf16[512,1024]{1,0:T(8,128)(2,1)S(1)}, bf16[512,1024]{1,0:T(8,128)(2,1)}, u32[]{:S(2)}, u32[]{:S(2)}) collective-permute-start(bf16[512,1024]{1,0:T(8,128)(2,1)S(1)} %get-tuple-element.65), channel_id=1, source_target_pairs={{0,16},{4,20},{8,24},{12,28},{16,0},{20,4},{24,8},{28,12},{1,17},{... | collective-permute-start | bytes 3145736 | tf_op jit(solution)/shard_map/ppermute | solution.py:18
  385.8 87.1 %collective-permute-start.5 = (bf16[320,1024]{1,0:T(8,128)(2,1)S(1)}, bf16[320,1024]{1,0:T(8,128)(2,1)S(1)}, u32[]{:S(2)}, u32[]{:S(2)}) collective-permute-start(bf16[320,1024]{1,0:T(8,128)(2,1)S(1)} %get-tuple-element.127), channel_id=1, source_target_pairs={{0,2},{1,3},{2,0},{3,1},{4,6},{5,7},{6,4},{7,5},{8,10},{9,11},{10,... | collective-permute-start | bytes 1966088 | tf_op jit(solution)/shard_map/ppermute | solution.py:18
  387.3 85.6 %collective-permute-start.4 = (bf16[320,1024]{1,0:T(8,128)(2,1)S(1)}, bf16[320,1024]{1,0:T(8,128)(2,1)S(1)}, u32[]{:S(2)}, u32[]{:S(2)}) collective-permute-start(bf16[320,1024]{1,0:T(8,128)(2,1)S(1)} %get-tuple-element.127), channel_id=1, source_target_pairs={{0,1},{1,0},{2,3},{3,2},{4,5},{5,4},{6,7},{7,6},{8,9},{9,8},{10,11... | collective-permute-start | bytes 1966088 | tf_op jit(solution)/shard_map/ppermute | solution.py:18
  387.3 86.5 %collective-permute-start.6 = (bf16[320,1024]{1,0:T(8,128)(2,1)S(1)}, bf16[320,1024]{1,0:T(8,128)(2,1)S(1)}, u32[]{:S(2)}, u32[]{:S(2)}) collective-permute-start(bf16[320,1024]{1,0:T(8,128)(2,1)S(1)} %get-tuple-element.127), channel_id=1, source_target_pairs={{0,3},{1,2},{2,1},{3,0},{4,7},{5,6},{6,5},{7,4},{8,11},{9,10},{10,... | collective-permute-start | bytes 1966088 | tf_op jit(solution)/shard_map/ppermute | solution.py:18
  423.6 65.6 %collective-permute-start.12 = (bf16[512,1024]{1,0:T(8,128)(2,1)}, bf16[512,1024]{1,0:T(8,128)(2,1)}, u32[]{:S(2)}, u32[]{:S(2)}) collective-permute-start(bf16[512,1024]{1,0:T(8,128)(2,1)} %get-tuple-element.66), channel_id=1, source_target_pairs={{0,28},{4,24},{8,20},{12,16},{16,12},{20,8},{24,4},{28,0},{1,29},{... | collective-permute-start | bytes 3145736 | tf_op jit(solution)/shard_map/ppermute | solution.py:18
  469.8 28.2 %collective-permute-start.13 = (bf16[512,1024]{1,0:T(8,128)(2,1)}, bf16[512,1024]{1,0:T(8,128)(2,1)}, u32[]{:S(2)}, u32[]{:S(2)}) collective-permute-start(bf16[512,1024]{1,0:T(8,128)(2,1)} %get-tuple-element.67), channel_id=1, source_target_pairs={{0,24},{4,28},{8,16},{12,20},{16,8},{20,12},{24,0},{28,4},{1,25},{... | collective-permute-start | bytes 3145736 | tf_op jit(solution)/shard_map/ppermute | solution.py:18
  472.9 59.9 %collective-permute-start.23 = (bf16[512,1024]{1,0:T(8,128)(2,1)}, bf16[512,1024]{1,0:T(8,128)(2,1)S(1)}, u32[]{:S(2)}, u32[]{:S(2)}) collective-permute-start(bf16[512,1024]{1,0:T(8,128)(2,1)} %get-tuple-element.109), channel_id=1, source_target_pairs={{0,12},{4,8},{8,4},{12,0},{16,28},{20,24},{24,20},{28,16},{1,13},{... | collective-permute-start | bytes 3145736 | tf_op jit(solution)/shard_map/ppermute | solution.py:18
  473.8 79.6 %collective-permute-start.22 = (bf16[512,1024]{1,0:T(8,128)(2,1)}, bf16[512,1024]{1,0:T(8,128)(2,1)S(1)}, u32[]{:S(2)}, u32[]{:S(2)}) collective-permute-start(bf16[512,1024]{1,0:T(8,128)(2,1)} %get-tuple-element.110), channel_id=1, source_target_pairs={{0,4},{4,0},{8,12},{12,8},{16,20},{20,16},{24,28},{28,24},{1,5},{5... | collective-permute-start | bytes 3145736 | tf_op jit(solution)/shard_map/ppermute | solution.py:18
  474.9 80.4 %collective-permute-start.21 = (bf16[512,1024]{1,0:T(8,128)(2,1)}, bf16[512,1024]{1,0:T(8,128)(2,1)S(1)}, u32[]{:S(2)}, u32[]{:S(2)}) collective-permute-start(bf16[512,1024]{1,0:T(8,128)(2,1)} %get-tuple-element.111), channel_id=1, source_target_pairs={{0,8},{4,12},{8,0},{12,4},{16,24},{20,28},{24,16},{28,20},{1,9},{5... | collective-permute-start | bytes 3145736 | tf_op jit(solution)/shard_map/ppermute | solution.py:18
  489.2 121.3 %collective-permute-start.40 = (bf16[128,1024]{1,0:T(8,128)(2,1)}, bf16[128,1024]{1,0:T(8,128)(2,1)S(1)}, u32[]{:S(2)}, u32[]{:S(2)}) collective-permute-start(bf16[128,1024]{1,0:T(8,128)(2,1)} %get-tuple-element.112), channel_id=1, source_target_pairs={{0,28},{4,24},{8,20},{12,16},{16,12},{20,8},{24,4},{28,0},{1,29},{... | collective-permute-start | bytes 786440 | tf_op jit(solution)/shard_map/ppermute | solution.py:18
  497.9 112.6 %collective-permute-start.41 = (bf16[128,1024]{1,0:T(8,128)(2,1)}, bf16[128,1024]{1,0:T(8,128)(2,1)}, u32[]{:S(2)}, u32[]{:S(2)}) collective-permute-start(bf16[128,1024]{1,0:T(8,128)(2,1)} %get-tuple-element.113), channel_id=1, source_target_pairs={{0,24},{4,28},{8,16},{12,20},{16,8},{20,12},{24,0},{28,4},{1,25},{... | collective-permute-start | bytes 786440 | tf_op jit(solution)/shard_map/ppermute | solution.py:18
  532.8 25.9 %copy-start = (bf16[512,1024]{1,0:T(8,128)(2,1)}, bf16[512,1024]{1,0:T(8,128)(2,1)S(1)}, u32[]{:S(2)}) copy-start(bf16[512,1024]{1,0:T(8,128)(2,1)S(1)} %collective-permute-done.23.refs_6_) | copy-start | bytes 3145732
  532.8 77.7 %collective-permute-start.38 = (bf16[128,1024]{1,0:T(8,128)(2,1)}, bf16[128,1024]{1,0:T(8,128)(2,1)}, u32[]{:S(2)}, u32[]{:S(2)}) collective-permute-start(bf16[128,1024]{1,0:T(8,128)(2,1)} %get-tuple-element.114), channel_id=1, source_target_pairs={{0,20},{4,16},{8,28},{12,24},{16,4},{20,0},{24,12},{28,8},{1,21},{... | collective-permute-start | bytes 786440 | tf_op jit(solution)/shard_map/ppermute | solution.py:18
  553.4 57.1 %collective-permute-start.39 = (bf16[128,1024]{1,0:T(8,128)(2,1)}, bf16[128,1024]{1,0:T(8,128)(2,1)}, u32[]{:S(2)}, u32[]{:S(2)}) collective-permute-start(bf16[128,1024]{1,0:T(8,128)(2,1)} %get-tuple-element.115), channel_id=1, source_target_pairs={{0,16},{4,20},{8,24},{12,28},{16,0},{20,4},{24,8},{28,12},{1,17},{... | collective-permute-start | bytes 786440 | tf_op jit(solution)/shard_map/ppermute | solution.py:18
  555.3 50.6 %collective-permute-start.32 = (bf16[128,1024]{1,0:T(8,128)(2,1)}, bf16[128,1024]{1,0:T(8,128)(2,1)}, u32[]{:S(2)}, u32[]{:S(2)}) collective-permute-start(bf16[128,1024]{1,0:T(8,128)(2,1)} %get-tuple-element.119), channel_id=1, source_target_pairs={{0,16},{4,20},{8,24},{12,28},{16,0},{20,4},{24,8},{28,12},{1,17},{... | collective-permute-start | bytes 786440 | tf_op jit(solution)/shard_map/ppermute | solution.py:18
  610.4 8.1 %collective-permute-start.35 = (bf16[320,256]{1,0:T(8,128)(2,1)}, bf16[320,256]{1,0:T(8,128)(2,1)S(1)}, u32[]{:S(2)}, u32[]{:S(2)}) collective-permute-start(bf16[320,256]{1,0:T(8,128)(2,1)} %get-tuple-element.85), channel_id=1, source_target_pairs={{0,1},{1,0},{2,3},{3,2},{4,5},{5,4},{6,7},{7,6},{8,9},{9,8},{10,11... | collective-permute-start | bytes 491528 | tf_op jit(solution)/shard_map/ppermute | solution.py:18
  611.2 8.9 %copy-start.29 = (bf16[320,512]{1,0:T(8,128)(2,1)S(1)}, bf16[320,512]{1,0:T(8,128)(2,1)}, u32[]{:S(2)}) copy-start(bf16[320,512]{1,0:T(8,128)(2,1)} %get-tuple-element.82) | copy-start | bytes 983044
  611.2 35.3 %copy-start.25 = (bf16[320,256]{1,0:T(8,128)(2,1)S(1)}, bf16[320,256]{1,0:T(8,128)(2,1)}, u32[]{:S(2)}) copy-start(bf16[320,256]{1,0:T(8,128)(2,1)} %get-tuple-element.84) | copy-start | bytes 491524
  615.8 30.8 %copy-start.20 = (bf16[320,512]{1,0:T(8,128)(2,1)S(1)}, bf16[320,512]{1,0:T(8,128)(2,1)}, u32[]{:S(2)}) copy-start(bf16[320,512]{1,0:T(8,128)(2,1)} %get-tuple-element.79) | copy-start | bytes 983044
  615.8 4.2 collective-permute-start.42
  616.4 7.3 %collective-permute-start.43 = (bf16[320,256]{1,0:T(8,128)(2,1)}, bf16[320,256]{1,0:T(8,128)(2,1)S(1)}, u32[]{:S(2)}, u32[]{:S(2)}) collective-permute-start(bf16[320,256]{1,0:T(8,128)(2,1)} %get-tuple-element.91), channel_id=1, source_target_pairs={{0,2},{1,3},{2,0},{3,1},{4,6},{5,7},{6,4},{7,5},{8,10},{9,11},{10,... | collective-permute-start | bytes 491528 | tf_op jit(solution)/shard_map/ppermute | solution.py:18
  617.9 8.4 %collective-permute-start.44 = (bf16[320,256]{1,0:T(8,128)(2,1)}, bf16[320,256]{1,0:T(8,128)(2,1)S(1)}, u32[]{:S(2)}, u32[]{:S(2)}) collective-permute-start(bf16[320,256]{1,0:T(8,128)(2,1)} %get-tuple-element.92), channel_id=1, source_target_pairs={{0,3},{1,2},{2,1},{3,0},{4,7},{5,6},{6,5},{7,4},{8,11},{9,10},{10,... | collective-permute-start | bytes 491528 | tf_op jit(solution)/shard_map/ppermute | solution.py:18
  617.9 28.7 %collective-permute-start.28 = (bf16[320,512]{1,0:T(8,128)(2,1)S(1)}, bf16[320,512]{1,0:T(8,128)(2,1)S(1)}, u32[]{:S(2)}, u32[]{:S(2)}) collective-permute-start(bf16[320,512]{1,0:T(8,128)(2,1)S(1)} %copy-done.31), channel_id=1, source_target_pairs={{0,1},{1,0},{2,3},{3,2},{4,5},{5,4},{6,7},{7,6},{8,9},{9,8},{10,11... | collective-permute-start | bytes 983048 | tf_op jit(solution)/shard_map/ppermute | solution.py:18
  618.5 28.1 %collective-permute-start.29 = (bf16[320,512]{1,0:T(8,128)(2,1)S(1)}, bf16[320,512]{1,0:T(8,128)(2,1)S(1)}, u32[]{:S(2)}, u32[]{:S(2)}) collective-permute-start(bf16[320,512]{1,0:T(8,128)(2,1)S(1)} %copy-done.30), channel_id=1, source_target_pairs={{0,2},{1,3},{2,0},{3,1},{4,6},{5,7},{6,4},{7,5},{8,10},{9,11},{10,... | collective-permute-start | bytes 983048 | tf_op jit(solution)/shard_map/ppermute | solution.py:18
  620.1 26.6 %collective-permute-start.30 = (bf16[320,512]{1,0:T(8,128)(2,1)S(1)}, bf16[320,512]{1,0:T(8,128)(2,1)S(1)}, u32[]{:S(2)}, u32[]{:S(2)}) collective-permute-start(bf16[320,512]{1,0:T(8,128)(2,1)S(1)} %copy-done.29), channel_id=1, source_target_pairs={{0,3},{1,2},{2,1},{3,0},{4,7},{5,6},{6,5},{7,4},{8,11},{9,10},{10,... | collective-permute-start | bytes 983048 | tf_op jit(solution)/shard_map/ppermute | solution.py:18
  623.7 21.1 %collective-permute-start.36 = (bf16[320,256]{1,0:T(8,128)(2,1)}, bf16[320,256]{1,0:T(8,128)(2,1)S(1)}, u32[]{:S(2)}, u32[]{:S(2)}) collective-permute-start(bf16[320,256]{1,0:T(8,128)(2,1)} %get-tuple-element.86), channel_id=1, source_target_pairs={{0,2},{1,3},{2,0},{3,1},{4,6},{5,7},{6,4},{7,5},{8,10},{9,11},{10,... | collective-permute-start | bytes 491528 | tf_op jit(solution)/shard_map/ppermute | solution.py:18
  626.3 20.2 %collective-permute-start.37 = (bf16[320,256]{1,0:T(8,128)(2,1)}, bf16[320,256]{1,0:T(8,128)(2,1)S(1)}, u32[]{:S(2)}, u32[]{:S(2)}) collective-permute-start(bf16[320,256]{1,0:T(8,128)(2,1)} %get-tuple-element.87), channel_id=1, source_target_pairs={{0,3},{1,2},{2,1},{3,0},{4,7},{5,6},{6,5},{7,4},{8,11},{9,10},{10,... | collective-permute-start | bytes 491528 | tf_op jit(solution)/shard_map/ppermute | solution.py:18
  629.8 17.9 %all-to-all-start.1 = ((bf16[8,40,256]{2,1,0:T(8,128)(2,1)}), bf16[8,40,256]{2,1,0:T(8,128)(2,1)S(1)}, u32[]{:S(2)}, u32[]{:S(2)}) async-start(bf16[8,40,256]{2,1,0:T(8,128)(2,1)} %bitcast.55), calls=%async_computation.1 | async-start | bytes 327680 | tf_op jit(solution)/shard_map/all_to_all | solution.py:276
  647.7 18.4 %all-to-all-start = ((bf16[8,40,768]{2,1,0:T(8,128)(2,1)}), bf16[8,40,768]{2,1,0:T(8,128)(2,1)S(1)}, u32[]{:S(2)}, u32[]{:S(2)}) async-start(bf16[8,40,768]{2,1,0:T(8,128)(2,1)} %pad_maximum_fusion.3), calls=%async_computation | async-start | bytes 983040 | tf_op jit(solution)/shard_map/all_to_all | solution.py:276
  (15 other events, 38.2 us)
where the time goes:
time: 668 us; the launch traced here: 667 us
  waiting for transfers between devices  325 us (49%)
  starting transfers between devices  246 us (37%)
  Pallas kernels  34.7 us (5%)
  other arithmetic  34.2 us (5%)
  local copies, waits for them, and re-layouts  26.1 us (4%)
    ppermute x45, waiting for transfers between devices, swap(): return lax.ppermute(value, axis, [(i, i ^ k) for i in range(count)])  310 us
    ppermute x45, starting transfers between devices, swap(): return lax.ppermute(value, axis, [(i, i ^ k) for i in range(count)])  239 us
    convert_element_type x4, other arithmetic, make_piece(): return piece.astype(jnp.bfloat16)  23.9 us
    pallas_call x2, Pallas kernels, activate(): pl.pallas_call(functools.partial(act_kernel, count, per_tp, keys, gate is...  18.9 us
    pallas_call x3, Pallas kernels, down_partial(): pl.pallas_call(functools.partial(down_kernel, keys, offsets, rows, width,...  15.7 us
    all_to_all x2, waiting for transfers between devices, per_device(): back = lax.all_to_all(away, 'fs', split_axis=0, concat_axis=0, tiled=True)  14.8 us
    convert_element_type x4, local copies, waits for them, and re-layouts, make_piece(): return piece.astype(jnp.bfloat16)  14.5 us
  transfers between devices with their start and end apart: 47, of which 18 were waited for; matrix products, arithmetic and copies ran while one was open for 8% of the time, Pallas kernels for 5%

commit v1 on v0

--- a/solution.py
+++ b/solution.py
@@ -7,6 +7,8 @@
 from jax.experimental.pallas import tpu as pltpu
 from jax.sharding import PartitionSpec as P
 
+
+CAP = 30
 
 HBM = pltpu.MemorySpace.HBM
 VMEM = pltpu.MemorySpace.VMEM
@@ -101,61 +103,100 @@
     )(*args)
 
 
-def down_kernel(keys, offsets, rows, width, start, aliased, *refs):
-    me_ref, hidden_ref, weight_ref = refs[:3]
-    count = len(keys)
-    pieces = refs[3 : 3 + count]
-    refs = refs[3 + count + aliased :]
-    out_ref, blocks = refs[0], refs[1:-3]
-    held, load_sem, place_sem = refs[-3:]
+def fetch(keys, offsets, rows, width, start, me_ref, pieces, out_ref, held, load_sem, place_sem):
     loads, places = [], []
-    for j in range(count):
+    for j in range(len(keys)):
         slot = me_ref[0] ^ keys[j]
         spot = held.at[pl.ds(pl.multiple_of(slot * rows, rows), rows)]
-        first = pl.multiple_of(slot * width + start, 16)
         piece = pieces[j].at[pl.ds(offsets[j], rows)]
         loads.append(pltpu.make_async_copy(piece, spot, load_sem.at[j]))
-        places.append(
-            pltpu.make_async_copy(spot, out_ref.at[pl.ds(first, rows)], place_sem.at[j])
+        if out_ref is not None:
+            first = pl.multiple_of(slot * width + start, 16)
+            places.append(
+                pltpu.make_async_copy(spot, out_ref.at[pl.ds(first, rows)], place_sem.at[j])
+            )
+    return loads, places
+
+
+def down_kernel(keys, offsets, rows, me_ref, hidden_ref, *refs):
+    pieces, blocks = refs[: len(keys)], refs[len(keys) : -6]
+    hidden, held, sums, hidden_sem, load_sem, store_sem = refs[-6:]
+    loads, _ = fetch(keys, offsets, rows, 0, 0, me_ref, pieces, None, held, load_sem, None)
+    loads.append(pltpu.make_async_copy(hidden_ref, hidden, hidden_sem))
+    for load in loads:
+        load.start()
+    for load in loads:
+        load.wait()
+    span = held.shape[0] // len(blocks)
+    stores = []
+    for rel in reversed(range(len(blocks))):
+        block = me_ref[1] ^ rel
+        part = lax.dot_general(
+            hidden[...],
+            held[pl.ds(pl.multiple_of(block * span, span), span)],
+            (((1,), (1,)), ((), ())),
+            preferred_element_type=jnp.float32,
         )
+        sums[rel] = part.astype(jnp.bfloat16)
+        store = pltpu.make_async_copy(sums.at[rel], blocks[rel], store_sem.at[rel])
+        store.start()
+        stores.append(store)
+    for store in stores:
+        store.wait()
+
+
+def down_partial(me, hidden, pieces, keys, parts, width, start, rows):
+    count = len(pieces)
+    columns = pieces[0].shape[1]
+    offsets = [start if piece.shape[0] == width else 0 for piece in pieces]
+    block = jax.ShapeDtypeStruct((hidden.shape[0], count * rows // parts), jnp.bfloat16)
+    return pl.pallas_call(
+        functools.partial(down_kernel, keys, offsets, rows),
+        in_specs=[pl.BlockSpec(memory_space=SMEM)]
+        + [pl.BlockSpec(memory_space=HBM)] * (1 + count),
+        out_specs=[pl.BlockSpec(memory_space=HBM)] * parts,
+        out_shape=[block] * parts,
+        scratch_shapes=[
+            pltpu.VMEM(hidden.shape, jnp.bfloat16),
+            pltpu.VMEM((count * rows, columns), jnp.bfloat16),
+            pltpu.VMEM((parts,) + block.shape, jnp.bfloat16),
+            pltpu.SemaphoreType.DMA,
+            pltpu.SemaphoreType.DMA((count,)),
+            pltpu.SemaphoreType.DMA((parts,)),
+        ],
+    )(me, hidden, *pieces)
+
+
+def place_kernel(keys, offsets, rows, width, start, aliased, me_ref, *refs):
+    pieces = refs[: len(keys)]
+    out_ref, held, load_sem, place_sem = refs[len(keys) + aliased :]
+    loads, places = fetch(
+        keys, offsets, rows, width, start, me_ref, pieces, out_ref, held, load_sem, place_sem
+    )
     for load in loads:
         load.start()
     for load, place in zip(loads, places):
         load.wait()
         place.start()
-    span = held.shape[0] // len(blocks)
-    for rel, block_ref in enumerate(blocks):
-        block = me_ref[1] ^ rel
-        part = lax.dot_general(
-            hidden_ref[...],
-            held[pl.ds(pl.multiple_of(block * span, span), span)],
-            (((1,), (1,)), ((), ())),
-            preferred_element_type=jnp.float32,
-        )
-        block_ref[...] = (part * weight_ref[...]).astype(jnp.bfloat16)
     for place in places:
         place.wait()
 
 
-def down_partial(me, hidden, weight, pieces, keys, parts, width, start, rows, out):
+def place_chunk(me, pieces, keys, width, start, rows, out):
     count = len(pieces)
     columns = pieces[0].shape[1]
     offsets = [start if piece.shape[0] == width else 0 for piece in pieces]
-    tokens = hidden.shape[0]
-    block = jax.ShapeDtypeStruct((tokens, count * rows // parts), jnp.bfloat16)
-    args = [me, hidden, weight, *pieces]
-    in_specs = [pl.BlockSpec(memory_space=SMEM)] + [pl.BlockSpec(memory_space=VMEM)] * 2
-    in_specs += [pl.BlockSpec(memory_space=HBM)] * count
+    args = [me, *pieces]
     aliases = {}
     if out is not None:
         aliases = {len(args): 0}
         args.append(out)
-        in_specs.append(pl.BlockSpec(memory_space=HBM))
     return pl.pallas_call(
-        functools.partial(down_kernel, keys, offsets, rows, width, start, len(aliases)),
-        in_specs=in_specs,
-        out_specs=[pl.BlockSpec(memory_space=HBM)] + [pl.BlockSpec(memory_space=VMEM)] * parts,
-        out_shape=[jax.ShapeDtypeStruct((count * width, columns), jnp.bfloat16)] + [block] * parts,
+        functools.partial(place_kernel, keys, offsets, rows, width, start, len(aliases)),
+        in_specs=[pl.BlockSpec(memory_space=SMEM)]
+        + [pl.BlockSpec(memory_space=HBM)] * (len(args) - 1),
+        out_specs=pl.BlockSpec(memory_space=HBM),
+        out_shape=jax.ShapeDtypeStruct((count * width, columns), jnp.bfloat16),
         scratch_shapes=[
             pltpu.VMEM((count * rows, columns), jnp.bfloat16),
             pltpu.SemaphoreType.DMA((count,)),
@@ -172,7 +213,7 @@
     return stacked[jnp.take(where, index)]
 
 
-def make_packet(tokens, routes, route_logits, experts):
+def pack_rows(tokens, routes, route_logits, experts):
     tok_float = tokens.astype(jnp.float32)
     normed = (
         tok_float * lax.rsqrt(jnp.mean(tok_float * tok_float, axis=1, keepdims=True) + 1e-05)
@@ -181,15 +222,19 @@
     own_cols = lax.dynamic_slice_in_dim(normed, lax.axis_index("tp") * part_width, part_width, 1)
     shares = jax.nn.sigmoid(route_logits - route_logits[:, ::-1])
     expert_ids = lax.broadcasted_iota(jnp.int32, (1, 1, experts), 2)
-    weights = jnp.sum(jnp.where(routes[:, :, None] == expert_ids, shares[:, :, None], 0.0), axis=1)
-    terms, rest = [], weights
-    for _ in range(3):
-        term = lax.reduce_precision(rest, 8, 7)
-        terms.append(term.astype(jnp.bfloat16))
-        rest = rest - term
-    extra = jnp.concatenate(terms, axis=1)
-    extra = jnp.pad(extra, ((0, 0), (0, -extra.shape[1] % 128)))
-    return jnp.concatenate([own_cols, extra], axis=1)
+    picks = routes[:, :, None] == expert_ids
+    member = jnp.sum(picks.astype(jnp.int32), axis=1)
+    rows = lax.broadcasted_iota(jnp.int32, (1, tokens.shape[0]), 1)
+    earlier = jnp.transpose(rows) > rows
+    position = jnp.sum(jnp.where(earlier[:, :, None], member[None], 0), axis=1)
+    slots = -(-CAP // 16) * 16
+    slot_ids = lax.broadcasted_iota(jnp.int32, (1, 1, slots), 2)
+    placing = (position[:, :, None] == slot_ids) & (member[:, :, None] > 0)
+    packed = jnp.einsum(
+        "rec,rd->ecd", placing.astype(jnp.bfloat16), own_cols, preferred_element_type=jnp.float32
+    ).astype(jnp.bfloat16)
+    weights = jnp.sum(jnp.where(picks, shares[:, :, None], 0.0), axis=1)
+    return packed, jnp.where(placing, weights[:, :, None], 0.0)
 
 
 def per_device(tokens, routes, route_logits, norm_gain, gate_weight, up_weight, down_weight):
@@ -204,7 +249,7 @@
     me = jnp.stack([fs_me, tp_me]).astype(jnp.int32)
     near, far, first_order, order = partner_orders(fs_count, spread)
     keys = [0] + near + far
-    cuts = [0, width // 2, width * 3 // 4, width]
+    cuts = [0, width // 2, width * 3 // 4, width * 7 // 8, width]
     spans = [(start, end - start) for start, end in zip(cuts, cuts[1:])]
 
     def fold(weight, gain, k, start=0, rows=width):
@@ -220,10 +265,11 @@
     tokens, routes, route_logits, first = lax.optimization_barrier(
         (tokens, routes, route_logits, first)
     )
-    packet = make_packet(tokens, routes, route_logits, experts)
-    packet, gate_weight, first = lax.optimization_barrier((packet, gate_weight, first))
-    groups = list(range(spread, fs_count, spread))
-    held = [packet] + [swap(packet, "fs", k) for k in groups]
+    packed, combine = pack_rows(tokens, routes, route_logits, experts)
+    packed, gate_weight, first = lax.optimization_barrier((packed, gate_weight, first))
+    plane = lax.div(fs_me, spread)
+    packets = [lax.dynamic_index_in_dim(packed, plane ^ e, 0, False) for e in range(experts)]
+    held = packets[:1] + [swap(packets[e], "fs", e * spread) for e in range(1, experts)]
     gate_folds = {k: fold(gate_weight, norm_gain, k) for k in first_order[1:]}
     gate_folds, up_weight = lax.optimization_barrier((gate_folds, up_weight))
     gate_sent = send({first_order[0]: first, **gate_folds})
@@ -244,15 +290,10 @@
         for sent in down_sent
     ]
 
-    held = in_order(held, list(range(experts)), lax.div(fs_me, spread))
+    held = in_order(held, list(range(experts)), plane)
     held = [held] + [swap(held, "fs", k) for k in range(1, spread)]
     held = in_order(held, list(range(spread)), lax.rem(fs_me, spread))
-    gathered = jnp.swapaxes(held, 0, 1).reshape(fs_count * own_rows, packet.shape[1])
-    block = gathered[:, :part_width]
-    term_cols = gathered[:, part_width : part_width + 3 * experts].astype(jnp.float32)
-    row_weights = jnp.sum(term_cols.reshape(-1, 3, experts), axis=1)
-    mine = lax.broadcasted_iota(jnp.int32, (1, experts), 1) == lax.div(fs_me, spread)
-    row_weight = jnp.sum(jnp.where(mine, row_weights, 0.0), axis=1, keepdims=True)
+    block = jnp.swapaxes(held, 0, 1).reshape(-1, part_width)
     blocks = jnp.stack([block] + [swap(block, "tp", k) for k in range(1, tp_count)])
     x = blocks.reshape(tp_count, -1, per_tp, width)
     x = jnp.transpose(x, (0, 2, 1, 3)).reshape(fs_count, -1, width)
@@ -263,20 +304,23 @@
     down_out = None
     totals = []
     for span, pieces in zip(spans, down_pieces):
-        down_out, *parts = down_partial(
-            me, hidden, row_weight, pieces, keys, tp_count, width, *span, down_out
-        )
+        parts = down_partial(me, hidden, pieces, keys, tp_count, width, *span)
+        down_out = place_chunk(me, pieces, keys, width, *span, down_out)
         total = parts[0].astype(jnp.float32)
         for k in range(1, tp_count):
             total = total + swap(parts[k], "tp", k).astype(jnp.float32)
-        totals.append(total.astype(jnp.bfloat16).reshape(fs_count, own_rows, -1))
+        totals.append(total.astype(jnp.bfloat16).reshape(fs_count, -1, total.shape[1]))
+    combine = jnp.broadcast_to(
+        combine[:, :, None], (own_rows, experts, spread, combine.shape[2])
+    ).reshape(own_rows, -1)
     done = []
-    for group in [totals[:-1], totals[-1:]]:
+    for group in [totals[:2], totals[2:]]:
         away = jnp.concatenate(group, axis=2)
         back = lax.all_to_all(away, "fs", split_axis=0, concat_axis=0, tiled=True)
         ends = [part.shape[2] for part in group]
         ends = [sum(ends[: i + 1]) for i in range(len(ends) - 1)]
-        back = jnp.sum(back.astype(jnp.float32), axis=0).astype(jnp.bfloat16)
+        back = back.reshape(-1, back.shape[2]).astype(jnp.float32)
+        back = jnp.dot(combine, back, precision=lax.Precision.HIGHEST).astype(jnp.bfloat16)
         done += jnp.split(back, ends, axis=1)
     mixed = jnp.concatenate([part.reshape(own_rows, per_tp, -1) for part in done], axis=2)
     return mixed.reshape(own_rows, part_width), gate_out[None], up_out[None], down_out[None]

time: 668 us -> 641 us (0.960)
  waiting for transfers between devices: 325 us -> 268 us
  starting transfers between devices: 246 us -> 270 us
  Pallas kernels: 34.7 us -> 47 us
    ppermute x45 -> x52, waiting for transfers between devices: 310 us -> 268 us  [swap(): return lax.ppermute(value, axis, [(i, i ^ k) for i in range(count)])]
    ppermute x45 -> x52, starting transfers between devices: 239 us -> 261 us  [swap(): return lax.ppermute(value, axis, [(i, i ^ k) for i in range(count)])]
    all_to_all x2, waiting for transfers between devices: 14.8 us -> 0.01 us  [per_device(): back = lax.all_to_all(away, 'fs', split_axis=0, concat_axis=0, tiled=True)]
    pallas_call x3 -> x8, Pallas kernels: 15.7 us -> 28.9 us  [the longest x4 16 us: down_partial(): pl.pallas_call(functools.partial(down_kernel, keys, offsets, rows), in_sp...]
    convert_element_type x4 -> x5, local copies, waits for them, and re-layouts: 14.5 us -> 15.3 us  [make_piece(): return piece.astype(jnp.bfloat16)]
  transfers between devices with their start and end apart: 47 -> 54, of which waited for: 18 -> 19; matrix products, arithmetic and copies ran while one was open for 8% -> 8% of each run, Pallas kernels for 5% -> 7%
where the time goes in v1:
time: 641 us; the launch traced here: 640 us
  starting transfers between devices  270 us (42%)
  waiting for transfers between devices  268 us (42%)
  Pallas kernels  47 us (7%)
  other arithmetic  32.3 us (5%)
  local copies, waits for them, and re-layouts  20.3 us (3%)
    ppermute x52, waiting for transfers between devices, swap(): return lax.ppermute(value, axis, [(i, i ^ k) for i in range(count)])  268 us
    ppermute x52, starting transfers between devices, swap(): return lax.ppermute(value, axis, [(i, i ^ k) for i in range(count)])  261 us
    convert_element_type x4, other arithmetic, make_piece(): return piece.astype(jnp.bfloat16)  23.9 us
    pallas_call x2, Pallas kernels, activate(): pl.pallas_call(functools.partial(act_kernel, count, per_tp, keys, gate is...  18.1 us
    pallas_call x4, Pallas kernels, down_partial(): pl.pallas_call(functools.partial(down_kernel, keys, offsets, rows), in_sp...  16 us
    convert_element_type x5, local copies, waits for them, and re-layouts, make_piece(): return piece.astype(jnp.bfloat16)  15.3 us
    pallas_call x4, Pallas kernels, place_chunk(): pl.pallas_call(functools.partial(place_kernel, keys, offsets, rows, width...  12.8 us
  transfers between devices with their start and end apart: 54, of which 19 were waited for; matrix products, arithmetic and copies ran while one was open for 8% of the time, Pallas kernels for 7%

profile of v1, /device:TPU:0, one launch (start us, length us, event | category | flops | bytes accessed | tf_op | source)
XLA Modules:
  0.0 640.1 jit_solution(10601495101134228177)
XLA Ops:
  0.7 1.8 fusion.15
  3.3 5.1 collective-permute-start.2
  8.5 8.6 %fusion.9 = (bf16[512,1024]{1,0:T(8,128)(2,1)}, bf16[512,1024]{1,0:T(8,128)(2,1)}, bf16[512,1024]{1,0:T(8,128)(2,1)}, bf16[512,1024]{1,0:T(8,128)(2,1)}, bf16[51...) fusion(f32[4,512,2048]{2,1,0:T(8,128)} %param.13, s32[]{:T(128)S(6)} %select_n.244, s32[]{:T(128)S(6)} %select_n.245, ...), kind=kLoop, calls=%fused_computation.25 | loop fusion | flops 6291456 | bytes 18876464 | tf_op jit(solution)/shard_map/convert_element_type | solution.py:37
  17.1 9.6 %fusion.2 = (bf16[512,1024]{1,0:T(8,128)(2,1)}, bf16[512,1024]{1,0:T(8,128)(2,1)}, bf16[512,1024]{1,0:T(8,128)(2,1)}, bf16[512,1024]{1,0:T(8,128)(2,1)}, bf16[51...) fusion(f32[4,512,2048]{2,1,0:T(8,128)} %param.14, s32[]{:T(128)S(6)} %select_n.244, ...), kind=kLoop, calls=%fused_computation.11 | loop fusion | flops 7340032 | bytes 22022200 | tf_op jit(solution)/shard_map/convert_element_type | solution.py:37
  26.7 1.7 fusion.36
  28.3 2.9 collective-permute-start.47
  31.2 1.9 collective-permute-start.48
  34.3 2.4 fusion.27
  40.1 2.4 collective-permute-done
  42.5 2.2 collective-permute-start.40
  44.6 2.6 collective-permute-start.41
  47.2 9.5 %collective-permute-start.38 = (bf16[64,1024]{1,0:T(8,128)(2,1)S(1)}, bf16[64,1024]{1,0:T(8,128)(2,1)S(1)}, u32[]{:S(2)}, u32[]{:S(2)}) collective-permute-start(bf16[64,1024]{1,0:T(8,128)(2,1)S(1)} %get-tuple-element.120), channel_id=1, source_target_pairs={{0,20},{4,16},{8,28},{12,24},{16,4},{20,0},{24,12},{28,8},{1,21},{... | collective-permute-start | bytes 393224 | tf_op jit(solution)/shard_map/ppermute | solution.py:20
  56.7 3.3 collective-permute-done.45.refs_4_
  61.9 4.6 collective-permute-done.46.refs_5_
  66.6 26.3 %collective-permute-start.14 = (bf16[512,1024]{1,0:T(8,128)(2,1)}, bf16[512,1024]{1,0:T(8,128)(2,1)}, u32[]{:S(2)}, u32[]{:S(2)}) collective-permute-start(bf16[512,1024]{1,0:T(8,128)(2,1)} %get-tuple-element.70), channel_id=1, source_target_pairs={{0,8},{4,12},{8,0},{12,4},{16,24},{20,28},{24,16},{28,20},{1,9},{5... | collective-permute-start | bytes 3145736 | tf_op jit(solution)/shard_map/ppermute | solution.py:20
  92.9 2.7 collective-permute-start.33
  95.6 2.4 collective-permute-done.38.refs_4_
  98.1 1.9 collective-permute-start.34
  101.5 5.9 collective-permute-done.3
  108.1 17.5 %collective-permute-done.33.refs_6_ = bf16[128,1024]{1,0:T(8,128)(2,1)S(1)} collective-permute-done((bf16[128,1024]{1,0:T(8,128)(2,1)}, bf16[128,1024]{1,0:T(8,128)(2,1)S(1)}, u32[]{:S(2)}, u32[]{:S(2)}) %collective-permute-start.33) | collective-permute-done | bytes 262176 | tf_op jit(solution)/shard_map/ppermute | solution.py:20
  125.6 23.5 %collective-permute-done.34.refs_7_ = bf16[128,1024]{1,0:T(8,128)(2,1)S(1)} collective-permute-done((bf16[128,1024]{1,0:T(8,128)(2,1)}, bf16[128,1024]{1,0:T(8,128)(2,1)S(1)}, u32[]{:S(2)}, u32[]{:S(2)}) %collective-permute-start.34) | collective-permute-done | bytes 262176 | tf_op jit(solution)/shard_map/ppermute | solution.py:20
  149.2 1.5 collective-permute-start.5
  150.7 5.4 collective-permute-done.31.refs_4_
  156.2 3.1 collective-permute-start.15
  159.3 1.7 collective-permute-done.5
  161.0 9.5 %collective-permute-start.16 = (bf16[512,1024]{1,0:T(8,128)(2,1)}, bf16[512,1024]{1,0:T(8,128)(2,1)S(1)}, u32[]{:S(2)}, u32[]{:S(2)}) collective-permute-start(bf16[512,1024]{1,0:T(8,128)(2,1)} %get-tuple-element.72), channel_id=1, source_target_pairs={{0,12},{4,8},{8,4},{12,0},{16,28},{20,24},{24,20},{28,16},{1,13},{... | collective-permute-start | bytes 3145736 | tf_op jit(solution)/shard_map/ppermute | solution.py:20
  170.5 2.7 collective-permute-start.17
  173.2 2.1 collective-permute-start.19
  175.3 1.7 collective-permute-start.20
  177.0 73.2 %collective-permute-done.15.refs_4_ = bf16[512,1024]{1,0:T(8,128)(2,1)S(1)} collective-permute-done((bf16[512,1024]{1,0:T(8,128)(2,1)}, bf16[512,1024]{1,0:T(8,128)(2,1)S(1)}, u32[]{:S(2)}, u32[]{:S(2)}) %collective-permute-start.15) | collective-permute-done | bytes 1048608 | tf_op jit(solution)/shard_map/ppermute | solution.py:20
  251.6 14.7 %collective-permute-done.17.refs_6_ = bf16[512,1024]{1,0:T(8,128)(2,1)S(1)} collective-permute-done((bf16[512,1024]{1,0:T(8,128)(2,1)}, bf16[512,1024]{1,0:T(8,128)(2,1)S(1)}, u32[]{:S(2)}, u32[]{:S(2)}) %collective-permute-start.17) | collective-permute-done | bytes 1048608 | tf_op jit(solution)/shard_map/ppermute | solution.py:20
  267.5 24.9 %collective-permute-start.10 = (bf16[512,1024]{1,0:T(8,128)(2,1)}, bf16[512,1024]{1,0:T(8,128)(2,1)S(1)}, u32[]{:S(2)}, u32[]{:S(2)}) collective-permute-start(bf16[512,1024]{1,0:T(8,128)(2,1)} %get-tuple-element.65), channel_id=1, source_target_pairs={{0,20},{4,16},{8,28},{12,24},{16,4},{20,0},{24,12},{28,8},{1,21},{... | collective-permute-start | bytes 3145736 | tf_op jit(solution)/shard_map/ppermute | solution.py:20
  292.5 77.1 %collective-permute-start.11 = (bf16[512,1024]{1,0:T(8,128)(2,1)}, bf16[512,1024]{1,0:T(8,128)(2,1)S(1)}, u32[]{:S(2)}, u32[]{:S(2)}) collective-permute-start(bf16[512,1024]{1,0:T(8,128)(2,1)} %get-tuple-element.66), channel_id=1, source_target_pairs={{0,16},{4,20},{8,24},{12,28},{16,0},{20,4},{24,8},{28,12},{1,17},{... | collective-permute-start | bytes 3145736 | tf_op jit(solution)/shard_map/ppermute | solution.py:20
  369.6 1.8 collective-permute-start.12
  371.4 3.3 collective-permute-start.13
  374.7 4.7 fusion.19
  379.5 44.5 %collective-permute-done.10.refs_6_ = bf16[512,1024]{1,0:T(8,128)(2,1)S(1)} collective-permute-done((bf16[512,1024]{1,0:T(8,128)(2,1)}, bf16[512,1024]{1,0:T(8,128)(2,1)S(1)}, u32[]{:S(2)}, u32[]{:S(2)}) %collective-permute-start.10) | collective-permute-done | bytes 1048608 | tf_op jit(solution)/shard_map/ppermute | solution.py:20
  424.1 2.7 collective-permute-start.22
  426.7 20.9 %collective-permute-done.11.refs_7_ = bf16[512,1024]{1,0:T(8,128)(2,1)S(1)} collective-permute-done((bf16[512,1024]{1,0:T(8,128)(2,1)}, bf16[512,1024]{1,0:T(8,128)(2,1)S(1)}, u32[]{:S(2)}, u32[]{:S(2)}) %collective-permute-start.11) | collective-permute-done | bytes 1048608 | tf_op jit(solution)/shard_map/ppermute | solution.py:20
  448.7 3.7 fusion.23
  453.0 2.7 fusion.16.refs_0_
  455.7 3.9 fusion
  459.6 2.7 collective-permute-start.26
  463.5 1.6 pad_maximum_fusion
  465.1 53.9 %collective-permute-start.32 = (bf16[128,1024]{1,0:T(8,128)(2,1)}, bf16[128,1024]{1,0:T(8,128)(2,1)S(1)}, u32[]{:S(2)}, u32[]{:S(2)}) collective-permute-start(bf16[128,1024]{1,0:T(8,128)(2,1)} %get-tuple-element.125), channel_id=1, source_target_pairs={{0,16},{4,20},{8,24},{12,28},{16,0},{20,4},{24,8},{28,12},{1,17},{... | collective-permute-start | bytes 786440 | tf_op jit(solution)/shard_map/ppermute | solution.py:20
  519.0 2.6 collective-permute-start.25
  523.3 9.0 %shard_map.120 = (bf16[4096,1024]{1,0:T(8,128)(2,1)}, f32[256,1024]{1,0:T(8,128)}) custom-call(s32[2]{0:T(128)} %pad_add_fusion.refs_0_.me_ref, bf16[8,256,512]{2,1,0:T(8,128)(2,1)} %bitcast.159, bf16[512,1024]{1,0:T(8,128)(2,1)} %get-tuple-element.138.refs_2_, bf16[512,1024]{1,0:T(8,128)(2,1)} %collective-permute-done.14.refs_3_, ...), custom_call_target="tpu_custom_call" | custom-call | tf_op jit(solution)/shard_map/pallas_call | solution.py:89
  532.3 9.1 %shard_map.121 = (bf16[4096,1024]{1,0:T(8,128)(2,1)}, bf16[256,1024]{1,0:T(8,128)(2,1)}) custom-call(s32[2]{0:T(128)} %pad_add_fusion.refs_0_.me_ref, bf16[8,256,512]{2,1,0:T(8,128)(2,1)} %bitcast.160, bf16[512,1024]{1,0:T(8,128)(2,1)} %get-tuple-element.139.refs_2_, bf16[512,1024]{1,0:T(8,128)(2,1)} %collective-permute-done.7.refs_3_, ...), custom_call_target="tpu_custom_call" | custom-call | tf_op jit(solution)/shard_map/pallas_call | solution.py:89
  541.5 3.5 shard_map.125
  544.9 26.4 %collective-permute-done.32.refs_5_ = bf16[128,1024]{1,0:T(8,128)(2,1)S(1)} collective-permute-done((bf16[128,1024]{1,0:T(8,128)(2,1)}, bf16[128,1024]{1,0:T(8,128)(2,1)S(1)}, u32[]{:S(2)}, u32[]{:S(2)}) %collective-permute-start.32) | collective-permute-done | bytes 262176 | tf_op jit(solution)/shard_map/ppermute | solution.py:20
  571.4 1.8 collective-permute-start.51
  573.2 3.5 shard_map.124
  576.7 4.0 shard_map.123
  581.4 11.3 %collective-permute-done.25.refs_5_ = bf16[256,1024]{1,0:T(8,128)(2,1)} collective-permute-done((bf16[256,1024]{1,0:T(8,128)(2,1)}, bf16[256,1024]{1,0:T(8,128)(2,1)}, u32[]{:S(2)}, u32[]{:S(2)}) %collective-permute-start.25) | collective-permute-done | bytes 524320 | tf_op jit(solution)/shard_map/ppermute | solution.py:20
  593.2 5.1 shard_map.122
  598.4 1.7 collective-permute-start.35
  604.9 4.3 all-to-all-start.1
  609.2 5.7 collective-permute-done.29
  615.0 3.8 collective-permute-done.30
  620.7 4.6 all-to-all-start
  625.7 4.2 shard_map.126.refs_8_
  629.9 3.1 shard_map.127.refs_8_
  633.0 2.8 shard_map.128.refs_8_
  635.8 2.8 shard_map.129
  (197 shorter events, 26.2 us)
Async XLA Ops:
  3.3 34.8 %collective-permute-start.2 = (bf16[32,1024]{1,0:T(8,128)(2,1)S(1)}, bf16[32,1024]{1,0:T(8,128)(2,1)S(1)}, u32[]{:S(2)}, u32[]{:S(2)}) collective-permute-start(bf16[32,1024]{1,0:T(8,128)(2,1)S(1)} %get-tuple-element.133), channel_id=1, source_target_pairs={{0,24},{4,28},{8,16},{12,20},{16,8},{20,12},{24,0},{28,4},{1,25},{... | collective-permute-start | bytes 196616 | tf_op jit(solution)/shard_map/ppermute | solution.py:20
  8.5 31.1 %collective-permute-start.1 = (bf16[32,1024]{1,0:T(8,128)(2,1)S(1)}, bf16[32,1024]{1,0:T(8,128)(2,1)S(1)}, u32[]{:S(2)}, u32[]{:S(2)}) collective-permute-start(bf16[32,1024]{1,0:T(8,128)(2,1)S(1)} %get-tuple-element.134), channel_id=1, source_target_pairs={{0,16},{4,20},{8,24},{12,28},{16,0},{20,4},{24,8},{28,12},{1,17},{... | collective-permute-start | bytes 196616 | tf_op jit(solution)/shard_map/ppermute | solution.py:20
  28.3 16.3 %collective-permute-start.47 = (bf16[64,1024]{1,0:T(8,128)(2,1)S(1)}, bf16[64,1024]{1,0:T(8,128)(2,1)S(1)}, u32[]{:S(2)}, u32[]{:S(2)}) collective-permute-start(bf16[64,1024]{1,0:T(8,128)(2,1)S(1)} %get-tuple-element.114), channel_id=1, source_target_pairs={{0,28},{4,24},{8,20},{12,16},{16,12},{20,8},{24,4},{28,0},{1,29},{... | collective-permute-start | bytes 393224 | tf_op jit(solution)/shard_map/ppermute | solution.py:20
  31.2 16.0 %collective-permute-start.48 = (bf16[64,1024]{1,0:T(8,128)(2,1)S(1)}, bf16[64,1024]{1,0:T(8,128)(2,1)S(1)}, u32[]{:S(2)}, u32[]{:S(2)}) collective-permute-start(bf16[64,1024]{1,0:T(8,128)(2,1)S(1)} %get-tuple-element.115), channel_id=1, source_target_pairs={{0,24},{4,28},{8,16},{12,20},{16,8},{20,12},{24,0},{28,4},{1,25},{... | collective-permute-start | bytes 393224 | tf_op jit(solution)/shard_map/ppermute | solution.py:20
  33.2 26.9 %collective-permute-start.45 = (bf16[64,1024]{1,0:T(8,128)(2,1)S(1)}, bf16[64,1024]{1,0:T(8,128)(2,1)S(1)}, u32[]{:S(2)}, u32[]{:S(2)}) collective-permute-start(bf16[64,1024]{1,0:T(8,128)(2,1)S(1)} %get-tuple-element.116), channel_id=1, source_target_pairs={{0,20},{4,16},{8,28},{12,24},{16,4},{20,0},{24,12},{28,8},{1,21},{... | collective-permute-start | bytes 393224 | tf_op jit(solution)/shard_map/ppermute | solution.py:20
  38.1 4.3 collective-permute-start
  39.5 27.0 %collective-permute-start.46 = (bf16[64,1024]{1,0:T(8,128)(2,1)S(1)}, bf16[64,1024]{1,0:T(8,128)(2,1)S(1)}, u32[]{:S(2)}, u32[]{:S(2)}) collective-permute-start(bf16[64,1024]{1,0:T(8,128)(2,1)S(1)} %get-tuple-element.117), channel_id=1, source_target_pairs={{0,16},{4,20},{8,24},{12,28},{16,0},{20,4},{24,8},{28,12},{1,17},{... | collective-permute-start | bytes 393224 | tf_op jit(solution)/shard_map/ppermute | solution.py:20
  42.5 24.1 %collective-permute-start.40 = (bf16[64,1024]{1,0:T(8,128)(2,1)S(1)}, bf16[64,1024]{1,0:T(8,128)(2,1)S(1)}, u32[]{:S(2)}, u32[]{:S(2)}) collective-permute-start(bf16[64,1024]{1,0:T(8,128)(2,1)S(1)} %get-tuple-element.118), channel_id=1, source_target_pairs={{0,28},{4,24},{8,20},{12,16},{16,12},{20,8},{24,4},{28,0},{1,29},{... | collective-permute-start | bytes 393224 | tf_op jit(solution)/shard_map/ppermute | solution.py:20
  44.6 63.4 %copy-start.18 = (bf16[64,1024]{1,0:T(8,128)(2,1)}, bf16[64,1024]{1,0:T(8,128)(2,1)S(1)}, u32[]{:S(2)}) copy-start(bf16[64,1024]{1,0:T(8,128)(2,1)S(1)} %collective-permute-done.47.refs_6_) | copy-start | bytes 393220
  44.6 48.3 %collective-permute-start.41 = (bf16[64,1024]{1,0:T(8,128)(2,1)S(1)}, bf16[64,1024]{1,0:T(8,128)(2,1)S(1)}, u32[]{:S(2)}, u32[]{:S(2)}) collective-permute-start(bf16[64,1024]{1,0:T(8,128)(2,1)S(1)} %get-tuple-element.119), channel_id=1, source_target_pairs={{0,24},{4,28},{8,16},{12,20},{16,8},{20,12},{24,0},{28,4},{1,25},{... | collective-permute-start | bytes 393224 | tf_op jit(solution)/shard_map/ppermute | solution.py:20
  47.2 50.8 %collective-permute-start.38 = (bf16[64,1024]{1,0:T(8,128)(2,1)S(1)}, bf16[64,1024]{1,0:T(8,128)(2,1)S(1)}, u32[]{:S(2)}, u32[]{:S(2)}) collective-permute-start(bf16[64,1024]{1,0:T(8,128)(2,1)S(1)} %get-tuple-element.120), channel_id=1, source_target_pairs={{0,20},{4,16},{8,28},{12,24},{16,4},{20,0},{24,12},{28,8},{1,21},{... | collective-permute-start | bytes 393224 | tf_op jit(solution)/shard_map/ppermute | solution.py:20
  60.0 39.9 %collective-permute-start.39 = (bf16[64,1024]{1,0:T(8,128)(2,1)S(1)}, bf16[64,1024]{1,0:T(8,128)(2,1)S(1)}, u32[]{:S(2)}, u32[]{:S(2)}) collective-permute-start(bf16[64,1024]{1,0:T(8,128)(2,1)S(1)} %get-tuple-element.121), channel_id=1, source_target_pairs={{0,16},{4,20},{8,24},{12,28},{16,0},{20,4},{24,8},{28,12},{1,17},{... | collective-permute-start | bytes 393224 | tf_op jit(solution)/shard_map/ppermute | solution.py:20
  66.6 106.7 %collective-permute-start.18 = (bf16[512,1024]{1,0:T(8,128)(2,1)S(1)}, bf16[512,1024]{1,0:T(8,128)(2,1)}, u32[]{:S(2)}, u32[]{:S(2)}) collective-permute-start(bf16[512,1024]{1,0:T(8,128)(2,1)S(1)} %fusion.15), channel_id=1, source_target_pairs={{0,16},{4,20},{8,24},{12,28},{16,0},{20,4},{24,8},{28,12},{1,17},{... | collective-permute-start | bytes 3145736 | tf_op jit(solution)/shard_map/ppermute | solution.py:20
  66.6 108.8 %collective-permute-start.14 = (bf16[512,1024]{1,0:T(8,128)(2,1)}, bf16[512,1024]{1,0:T(8,128)(2,1)}, u32[]{:S(2)}, u32[]{:S(2)}) collective-permute-start(bf16[512,1024]{1,0:T(8,128)(2,1)} %get-tuple-element.70), channel_id=1, source_target_pairs={{0,8},{4,12},{8,0},{12,4},{16,24},{20,28},{24,16},{28,20},{1,9},{5... | collective-permute-start | bytes 3145736 | tf_op jit(solution)/shard_map/ppermute | solution.py:20
  92.9 32.7 %collective-permute-start.33 = (bf16[128,1024]{1,0:T(8,128)(2,1)}, bf16[128,1024]{1,0:T(8,128)(2,1)S(1)}, u32[]{:S(2)}, u32[]{:S(2)}) collective-permute-start(bf16[128,1024]{1,0:T(8,128)(2,1)} %get-tuple-element.122), channel_id=1, source_target_pairs={{0,28},{4,24},{8,20},{12,16},{16,12},{20,8},{24,4},{28,0},{1,29},{... | collective-permute-start | bytes 786440 | tf_op jit(solution)/shard_map/ppermute | solution.py:20
  98.1 51.1 %collective-permute-start.34 = (bf16[128,1024]{1,0:T(8,128)(2,1)}, bf16[128,1024]{1,0:T(8,128)(2,1)S(1)}, u32[]{:S(2)}, u32[]{:S(2)}) collective-permute-start(bf16[128,1024]{1,0:T(8,128)(2,1)} %get-tuple-element.123), channel_id=1, source_target_pairs={{0,24},{4,28},{8,16},{12,20},{16,8},{20,12},{24,0},{28,4},{1,25},{... | collective-permute-start | bytes 786440 | tf_op jit(solution)/shard_map/ppermute | solution.py:20
  99.9 7.4 %collective-permute-start.3 = (bf16[4,32,1024]{2,1,0:T(8,128)(2,1)S(1)}, bf16[4,32,1024]{2,1,0:T(8,128)(2,1)S(1)}, u32[]{:S(2)}, u32[]{:S(2)}) collective-permute-start(bf16[4,32,1024]{2,1,0:T(8,128)(2,1)S(1)} %gather_fusion.1), channel_id=1, source_target_pairs={{0,4},{4,0},{8,12},{12,8},{16,20},{20,16},{24,28},{28,24},{1,5},{5... | collective-permute-start | bytes 786440 | tf_op jit(solution)/shard_map/ppermute | solution.py:20
  107.4 48.8 %collective-permute-start.31 = (bf16[128,1024]{1,0:T(8,128)(2,1)S(1)}, bf16[128,1024]{1,0:T(8,128)(2,1)S(1)}, u32[]{:S(2)}, u32[]{:S(2)}) collective-permute-start(bf16[128,1024]{1,0:T(8,128)(2,1)S(1)} %get-tuple-element.124), channel_id=1, source_target_pairs={{0,20},{4,16},{8,28},{12,24},{16,4},{20,0},{24,12},{28,8},{1,21},{... | collective-permute-start | bytes 786440 | tf_op jit(solution)/shard_map/ppermute | solution.py:20
  125.6 253.8 %copy-start.6 = (bf16[128,1024]{1,0:T(8,128)(2,1)}, bf16[128,1024]{1,0:T(8,128)(2,1)S(1)}, u32[]{:S(2)}) copy-start(bf16[128,1024]{1,0:T(8,128)(2,1)S(1)} %collective-permute-done.33.refs_6_) | copy-start | bytes 786436
  125.6 323.0 %copy-start.30 = (f32[40,2]{0,1:T(2,128)S(1)}, f32[40,2]{0,1:T(2,128)}, u32[]{:S(2)}) copy-start(f32[40,2]{0,1:T(2,128)} %param.11) | copy-start | bytes 964
  125.6 30.5 %collective-permute-start.6 = (bf16[256,1024]{1,0:T(8,128)(2,1)S(1)}, bf16[256,1024]{1,0:T(8,128)(2,1)}, u32[]{:S(2)}, u32[]{:S(2)}) collective-permute-start(bf16[256,1024]{1,0:T(8,128)(2,1)S(1)} %bitcast.162), channel_id=1, source_target_pairs={{0,3},{1,2},{2,1},{3,0},{4,7},{5,6},{6,5},{7,4},{8,11},{9,10},{10,... | collective-permute-start | bytes 1572872 | tf_op jit(solution)/shard_map/ppermute | solution.py:20
  149.2 230.3 %copy-start.7 = (bf16[128,1024]{1,0:T(8,128)(2,1)}, bf16[128,1024]{1,0:T(8,128)(2,1)S(1)}, u32[]{:S(2)}) copy-start(bf16[128,1024]{1,0:T(8,128)(2,1)S(1)} %collective-permute-done.34.refs_7_) | copy-start | bytes 786436
  149.2 11.8 %collective-permute-start.5 = (bf16[256,1024]{1,0:T(8,128)(2,1)S(1)}, bf16[256,1024]{1,0:T(8,128)(2,1)}, u32[]{:S(2)}, u32[]{:S(2)}) collective-permute-start(bf16[256,1024]{1,0:T(8,128)(2,1)S(1)} %bitcast.163), channel_id=1, source_target_pairs={{0,2},{1,3},{2,0},{3,1},{4,6},{5,7},{6,4},{7,5},{8,10},{9,11},{10,... | collective-permute-start | bytes 1572872 | tf_op jit(solution)/shard_map/ppermute | solution.py:20
  156.2 223.3 %copy-start.8 = (bf16[128,1024]{1,0:T(8,128)(2,1)}, bf16[128,1024]{1,0:T(8,128)(2,1)S(1)}, u32[]{:S(2)}) copy-start(bf16[128,1024]{1,0:T(8,128)(2,1)S(1)} %collective-permute-done.31.refs_4_) | copy-start | bytes 786436
  156.2 14.3 %collective-permute-start.4 = (bf16[256,1024]{1,0:T(8,128)(2,1)S(1)}, bf16[256,1024]{1,0:T(8,128)(2,1)}, u32[]{:S(2)}, u32[]{:S(2)}) collective-permute-start(bf16[256,1024]{1,0:T(8,128)(2,1)S(1)} %bitcast.164), channel_id=1, source_target_pairs={{0,1},{1,0},{2,3},{3,2},{4,5},{5,4},{6,7},{7,6},{8,9},{9,8},{10,11... | collective-permute-start | bytes 1572872 | tf_op jit(solution)/shard_map/ppermute | solution.py:20
  156.2 94.0 %collective-permute-start.15 = (bf16[512,1024]{1,0:T(8,128)(2,1)}, bf16[512,1024]{1,0:T(8,128)(2,1)S(1)}, u32[]{:S(2)}, u32[]{:S(2)}) collective-permute-start(bf16[512,1024]{1,0:T(8,128)(2,1)} %get-tuple-element.71), channel_id=1, source_target_pairs={{0,4},{4,0},{8,12},{12,8},{16,20},{20,16},{24,28},{28,24},{1,5},{5... | collective-permute-start | bytes 3145736 | tf_op jit(solution)/shard_map/ppermute | solution.py:20
  161.0 89.2 %collective-permute-start.16 = (bf16[512,1024]{1,0:T(8,128)(2,1)}, bf16[512,1024]{1,0:T(8,128)(2,1)S(1)}, u32[]{:S(2)}, u32[]{:S(2)}) collective-permute-start(bf16[512,1024]{1,0:T(8,128)(2,1)} %get-tuple-element.72), channel_id=1, source_target_pairs={{0,12},{4,8},{8,4},{12,0},{16,28},{20,24},{24,20},{28,16},{1,13},{... | collective-permute-start | bytes 3145736 | tf_op jit(solution)/shard_map/ppermute | solution.py:20
  170.5 95.8 %collective-permute-start.17 = (bf16[512,1024]{1,0:T(8,128)(2,1)}, bf16[512,1024]{1,0:T(8,128)(2,1)S(1)}, u32[]{:S(2)}, u32[]{:S(2)}) collective-permute-start(bf16[512,1024]{1,0:T(8,128)(2,1)} %get-tuple-element.73), channel_id=1, source_target_pairs={{0,20},{4,16},{8,28},{12,24},{16,4},{20,0},{24,12},{28,8},{1,21},{... | collective-permute-start | bytes 3145736 | tf_op jit(solution)/shard_map/ppermute | solution.py:20
  173.2 94.3 %collective-permute-start.19 = (bf16[512,1024]{1,0:T(8,128)(2,1)}, bf16[512,1024]{1,0:T(8,128)(2,1)S(1)}, u32[]{:S(2)}, u32[]{:S(2)}) collective-permute-start(bf16[512,1024]{1,0:T(8,128)(2,1)} %get-tuple-element.75), channel_id=1, source_target_pairs={{0,28},{4,24},{8,20},{12,16},{16,12},{20,8},{24,4},{28,0},{1,29},{... | collective-permute-start | bytes 3145736 | tf_op jit(solution)/shard_map/ppermute | solution.py:20
  175.3 117.1 %collective-permute-start.20 = (bf16[512,1024]{1,0:T(8,128)(2,1)}, bf16[512,1024]{1,0:T(8,128)(2,1)S(1)}, u32[]{:S(2)}, u32[]{:S(2)}) collective-permute-start(bf16[512,1024]{1,0:T(8,128)(2,1)} %get-tuple-element.76), channel_id=1, source_target_pairs={{0,24},{4,28},{8,16},{12,20},{16,8},{20,12},{24,0},{28,4},{1,25},{... | collective-permute-start | bytes 3145736 | tf_op jit(solution)/shard_map/ppermute | solution.py:20
  250.2 119.4 %collective-permute-start.7 = (bf16[512,1024]{1,0:T(8,128)(2,1)}, bf16[512,1024]{1,0:T(8,128)(2,1)}, u32[]{:S(2)}, u32[]{:S(2)}) collective-permute-start(bf16[512,1024]{1,0:T(8,128)(2,1)} %get-tuple-element.62), channel_id=1, source_target_pairs={{0,8},{4,12},{8,0},{12,4},{16,24},{20,28},{24,16},{28,20},{1,9},{5... | collective-permute-start | bytes 3145736 | tf_op jit(solution)/shard_map/ppermute | solution.py:20
  250.2 121.2 %collective-permute-start.8 = (bf16[512,1024]{1,0:T(8,128)(2,1)}, bf16[512,1024]{1,0:T(8,128)(2,1)}, u32[]{:S(2)}, u32[]{:S(2)}) collective-permute-start(bf16[512,1024]{1,0:T(8,128)(2,1)} %get-tuple-element.63), channel_id=1, source_target_pairs={{0,4},{4,0},{8,12},{12,8},{16,20},{20,16},{24,28},{28,24},{1,5},{5... | collective-permute-start | bytes 3145736 | tf_op jit(solution)/shard_map/ppermute | solution.py:20
  266.3 103.3 %copy-start.15 = (bf16[512,1024]{1,0:T(8,128)(2,1)}, bf16[512,1024]{1,0:T(8,128)(2,1)S(1)}, u32[]{:S(2)}) copy-start(bf16[512,1024]{1,0:T(8,128)(2,1)S(1)} %collective-permute-done.17.refs_6_) | copy-start | bytes 3145732
  266.3 113.2 %collective-permute-start.9 = (bf16[512,1024]{1,0:T(8,128)(2,1)}, bf16[512,1024]{1,0:T(8,128)(2,1)S(1)}, u32[]{:S(2)}, u32[]{:S(2)}) collective-permute-start(bf16[512,1024]{1,0:T(8,128)(2,1)} %get-tuple-element.64), channel_id=1, source_target_pairs={{0,12},{4,8},{8,4},{12,0},{16,28},{20,24},{24,20},{28,16},{1,13},{... | collective-permute-start | bytes 3145736 | tf_op jit(solution)/shard_map/ppermute | solution.py:20
  267.5 102.1 %copy-start.16 = (bf16[512,1024]{1,0:T(8,128)(2,1)}, bf16[512,1024]{1,0:T(8,128)(2,1)S(1)}, u32[]{:S(2)}) copy-start(bf16[512,1024]{1,0:T(8,128)(2,1)S(1)} %collective-permute-done.19.refs_8_) | copy-start | bytes 3145732
  267.5 156.5 %collective-permute-start.10 = (bf16[512,1024]{1,0:T(8,128)(2,1)}, bf16[512,1024]{1,0:T(8,128)(2,1)S(1)}, u32[]{:S(2)}, u32[]{:S(2)}) collective-permute-start(bf16[512,1024]{1,0:T(8,128)(2,1)} %get-tuple-element.65), channel_id=1, source_target_pairs={{0,20},{4,16},{8,28},{12,24},{16,4},{20,0},{24,12},{28,8},{1,21},{... | collective-permute-start | bytes 3145736 | tf_op jit(solution)/shard_map/ppermute | solution.py:20
  292.5 78.9 %copy-start.17 = (bf16[512,1024]{1,0:T(8,128)(2,1)}, bf16[512,1024]{1,0:T(8,128)(2,1)S(1)}, u32[]{:S(2)}) copy-start(bf16[512,1024]{1,0:T(8,128)(2,1)S(1)} %collective-permute-done.20.refs_9_) | copy-start | bytes 3145732
  292.5 155.2 %collective-permute-start.11 = (bf16[512,1024]{1,0:T(8,128)(2,1)}, bf16[512,1024]{1,0:T(8,128)(2,1)S(1)}, u32[]{:S(2)}, u32[]{:S(2)}) collective-permute-start(bf16[512,1024]{1,0:T(8,128)(2,1)} %get-tuple-element.66), channel_id=1, source_target_pairs={{0,16},{4,20},{8,24},{12,28},{16,0},{20,4},{24,8},{28,12},{1,17},{... | collective-permute-start | bytes 3145736 | tf_op jit(solution)/shard_map/ppermute | solution.py:20
  369.6 90.1 %collective-permute-start.12 = (bf16[512,1024]{1,0:T(8,128)(2,1)}, bf16[512,1024]{1,0:T(8,128)(2,1)}, u32[]{:S(2)}, u32[]{:S(2)}) collective-permute-start(bf16[512,1024]{1,0:T(8,128)(2,1)} %get-tuple-element.67), channel_id=1, source_target_pairs={{0,28},{4,24},{8,20},{12,16},{16,12},{20,8},{24,4},{28,0},{1,29},{... | collective-permute-start | bytes 3145736 | tf_op jit(solution)/shard_map/ppermute | solution.py:20
  371.4 90.9 %collective-permute-start.13 = (bf16[512,1024]{1,0:T(8,128)(2,1)}, bf16[512,1024]{1,0:T(8,128)(2,1)}, u32[]{:S(2)}, u32[]{:S(2)}) collective-permute-start(bf16[512,1024]{1,0:T(8,128)(2,1)} %get-tuple-element.68), channel_id=1, source_target_pairs={{0,24},{4,28},{8,16},{12,20},{16,8},{20,12},{24,0},{28,4},{1,25},{... | collective-permute-start | bytes 3145736 | tf_op jit(solution)/shard_map/ppermute | solution.py:20
  379.5 68.2 %copy-start.10 = (bf16[512,1024]{1,0:T(8,128)(2,1)}, bf16[512,1024]{1,0:T(8,128)(2,1)S(1)}, u32[]{:S(2)}) copy-start(bf16[512,1024]{1,0:T(8,128)(2,1)S(1)} %collective-permute-done.9.refs_5_) | copy-start | bytes 3145732
  379.5 85.6 %collective-permute-start.23 = (bf16[512,1024]{1,0:T(8,128)(2,1)}, bf16[512,1024]{1,0:T(8,128)(2,1)S(1)}, u32[]{:S(2)}, u32[]{:S(2)}) collective-permute-start(bf16[512,1024]{1,0:T(8,128)(2,1)} %get-tuple-element.111), channel_id=1, source_target_pairs={{0,12},{4,8},{8,4},{12,0},{16,28},{20,24},{24,20},{28,16},{1,13},{... | collective-permute-start | bytes 3145736 | tf_op jit(solution)/shard_map/ppermute | solution.py:20
  424.1 94.9 %collective-permute-start.22 = (bf16[512,1024]{1,0:T(8,128)(2,1)}, bf16[512,1024]{1,0:T(8,128)(2,1)S(1)}, u32[]{:S(2)}, u32[]{:S(2)}) collective-permute-start(bf16[512,1024]{1,0:T(8,128)(2,1)} %get-tuple-element.112), channel_id=1, source_target_pairs={{0,4},{4,0},{8,12},{12,8},{16,20},{20,16},{24,28},{28,24},{1,5},{5... | collective-permute-start | bytes 3145736 | tf_op jit(solution)/shard_map/ppermute | solution.py:20
  448.7 70.3 %collective-permute-start.21 = (bf16[512,1024]{1,0:T(8,128)(2,1)}, bf16[512,1024]{1,0:T(8,128)(2,1)S(1)}, u32[]{:S(2)}, u32[]{:S(2)}) collective-permute-start(bf16[512,1024]{1,0:T(8,128)(2,1)} %get-tuple-element.113), channel_id=1, source_target_pairs={{0,8},{4,12},{8,0},{12,4},{16,24},{20,28},{24,16},{28,20},{1,9},{5... | collective-permute-start | bytes 3145736 | tf_op jit(solution)/shard_map/ppermute | solution.py:20
  459.6 111.7 %collective-permute-start.26 = (bf16[256,1024]{1,0:T(8,128)(2,1)}, bf16[256,1024]{1,0:T(8,128)(2,1)}, u32[]{:S(2)}, u32[]{:S(2)}) collective-permute-start(bf16[256,1024]{1,0:T(8,128)(2,1)} %get-tuple-element.126), channel_id=1, source_target_pairs={{0,28},{4,24},{8,20},{12,16},{16,12},{20,8},{24,4},{28,0},{1,29},{... | collective-permute-start | bytes 1572872 | tf_op jit(solution)/shard_map/ppermute | solution.py:20
  462.3 109.1 %collective-permute-start.27 = (bf16[256,1024]{1,0:T(8,128)(2,1)}, bf16[256,1024]{1,0:T(8,128)(2,1)}, u32[]{:S(2)}, u32[]{:S(2)}) collective-permute-start(bf16[256,1024]{1,0:T(8,128)(2,1)} %get-tuple-element.127), channel_id=1, source_target_pairs={{0,24},{4,28},{8,16},{12,20},{16,8},{20,12},{24,0},{28,4},{1,25},{... | collective-permute-start | bytes 1572872 | tf_op jit(solution)/shard_map/ppermute | solution.py:20
  465.1 56.7 %copy-start = (bf16[512,1024]{1,0:T(8,128)(2,1)}, bf16[512,1024]{1,0:T(8,128)(2,1)S(1)}, u32[]{:S(2)}) copy-start(bf16[512,1024]{1,0:T(8,128)(2,1)S(1)} %collective-permute-done.23.refs_3_) | copy-start | bytes 3145732
  465.1 106.2 %collective-permute-start.32 = (bf16[128,1024]{1,0:T(8,128)(2,1)}, bf16[128,1024]{1,0:T(8,128)(2,1)S(1)}, u32[]{:S(2)}, u32[]{:S(2)}) collective-permute-start(bf16[128,1024]{1,0:T(8,128)(2,1)} %get-tuple-element.125), channel_id=1, source_target_pairs={{0,16},{4,20},{8,24},{12,28},{16,0},{20,4},{24,8},{28,12},{1,17},{... | collective-permute-start | bytes 786440 | tf_op jit(solution)/shard_map/ppermute | solution.py:20
  519.0 62.5 %collective-permute-start.24 = (bf16[256,1024]{1,0:T(8,128)(2,1)}, bf16[256,1024]{1,0:T(8,128)(2,1)}, u32[]{:S(2)}, u32[]{:S(2)}) collective-permute-start(bf16[256,1024]{1,0:T(8,128)(2,1)} %get-tuple-element.128), channel_id=1, source_target_pairs={{0,20},{4,16},{8,28},{12,24},{16,4},{20,0},{24,12},{28,8},{1,21},{... | collective-permute-start | bytes 1572872 | tf_op jit(solution)/shard_map/ppermute | solution.py:20
  519.0 73.7 %collective-permute-start.25 = (bf16[256,1024]{1,0:T(8,128)(2,1)}, bf16[256,1024]{1,0:T(8,128)(2,1)}, u32[]{:S(2)}, u32[]{:S(2)}) collective-permute-start(bf16[256,1024]{1,0:T(8,128)(2,1)} %get-tuple-element.129), channel_id=1, source_target_pairs={{0,16},{4,20},{8,24},{12,28},{16,0},{20,4},{24,8},{28,12},{1,17},{... | collective-permute-start | bytes 1572872 | tf_op jit(solution)/shard_map/ppermute | solution.py:20
  571.3 27.0 %collective-permute-start.49 = (bf16[256,128]{1,0:T(8,128)(2,1)}, bf16[256,128]{1,0:T(8,128)(2,1)S(1)}, u32[]{:S(2)}, u32[]{:S(2)}) collective-permute-start(bf16[256,128]{1,0:T(8,128)(2,1)} %get-tuple-element.93), channel_id=1, source_target_pairs={{0,1},{1,0},{2,3},{3,2},{4,5},{5,4},{6,7},{7,6},{8,9},{9,8},{10,11... | collective-permute-start | bytes 196616 | tf_op jit(solution)/shard_map/ppermute | solution.py:20
  571.3 27.1 %collective-permute-start.50 = (bf16[256,128]{1,0:T(8,128)(2,1)}, bf16[256,128]{1,0:T(8,128)(2,1)S(1)}, u32[]{:S(2)}, u32[]{:S(2)}) collective-permute-start(bf16[256,128]{1,0:T(8,128)(2,1)} %get-tuple-element.94), channel_id=1, source_target_pairs={{0,2},{1,3},{2,0},{3,1},{4,6},{5,7},{6,4},{7,5},{8,10},{9,11},{10,... | collective-permute-start | bytes 196616 | tf_op jit(solution)/shard_map/ppermute | solution.py:20
  571.4 28.8 %collective-permute-start.51 = (bf16[256,128]{1,0:T(8,128)(2,1)}, bf16[256,128]{1,0:T(8,128)(2,1)S(1)}, u32[]{:S(2)}, u32[]{:S(2)}) collective-permute-start(bf16[256,128]{1,0:T(8,128)(2,1)} %get-tuple-element.95), channel_id=1, source_target_pairs={{0,3},{1,2},{2,1},{3,0},{4,7},{5,6},{6,5},{7,4},{8,11},{9,10},{10,... | collective-permute-start | bytes 196616 | tf_op jit(solution)/shard_map/ppermute | solution.py:20
  581.4 19.2 %collective-permute-start.42 = (bf16[256,128]{1,0:T(8,128)(2,1)S(1)}, bf16[256,128]{1,0:T(8,128)(2,1)S(1)}, u32[]{:S(2)}, u32[]{:S(2)}) collective-permute-start(bf16[256,128]{1,0:T(8,128)(2,1)S(1)} %copy-done.38), channel_id=1, source_target_pairs={{0,1},{1,0},{2,3},{3,2},{4,5},{5,4},{6,7},{7,6},{8,9},{9,8},{10,11... | collective-permute-start | bytes 196616 | tf_op jit(solution)/shard_map/ppermute | solution.py:20
  592.8 9.0 %collective-permute-start.43 = (bf16[256,128]{1,0:T(8,128)(2,1)S(1)}, bf16[256,128]{1,0:T(8,128)(2,1)S(1)}, u32[]{:S(2)}, u32[]{:S(2)}) collective-permute-start(bf16[256,128]{1,0:T(8,128)(2,1)S(1)} %copy-done.37), channel_id=1, source_target_pairs={{0,2},{1,3},{2,0},{3,1},{4,6},{5,7},{6,4},{7,5},{8,10},{9,11},{10,... | collective-permute-start | bytes 196616 | tf_op jit(solution)/shard_map/ppermute | solution.py:20
  598.3 4.3 collective-permute-start.44
  598.4 5.4 collective-permute-start.35
  600.2 8.9 %collective-permute-start.36 = (bf16[256,256]{1,0:T(8,128)(2,1)S(1)}, bf16[256,256]{1,0:T(8,128)(2,1)S(1)}, u32[]{:S(2)}, u32[]{:S(2)}) collective-permute-start(bf16[256,256]{1,0:T(8,128)(2,1)S(1)} %copy-done.34), channel_id=1, source_target_pairs={{0,2},{1,3},{2,0},{3,1},{4,6},{5,7},{6,4},{7,5},{8,10},{9,11},{10,... | collective-permute-start | bytes 393224 | tf_op jit(solution)/shard_map/ppermute | solution.py:20
  600.6 8.5 %collective-permute-start.37 = (bf16[256,256]{1,0:T(8,128)(2,1)S(1)}, bf16[256,256]{1,0:T(8,128)(2,1)S(1)}, u32[]{:S(2)}, u32[]{:S(2)}) collective-permute-start(bf16[256,256]{1,0:T(8,128)(2,1)S(1)} %copy-done.33), channel_id=1, source_target_pairs={{0,3},{1,2},{2,1},{3,0},{4,7},{5,6},{6,5},{7,4},{8,11},{9,10},{10,... | collective-permute-start | bytes 393224 | tf_op jit(solution)/shard_map/ppermute | solution.py:20
  601.7 7.5 %collective-permute-start.28 = (bf16[256,512]{1,0:T(8,128)(2,1)}, bf16[256,512]{1,0:T(8,128)(2,1)S(1)}, u32[]{:S(2)}, u32[]{:S(2)}) collective-permute-start(bf16[256,512]{1,0:T(8,128)(2,1)} %get-tuple-element.81), channel_id=1, source_target_pairs={{0,1},{1,0},{2,3},{3,2},{4,5},{5,4},{6,7},{7,6},{8,9},{9,8},{10,11... | collective-permute-start | bytes 786440 | tf_op jit(solution)/shard_map/ppermute | solution.py:20
  602.6 12.4 %collective-permute-start.29 = (bf16[256,512]{1,0:T(8,128)(2,1)}, bf16[256,512]{1,0:T(8,128)(2,1)S(1)}, u32[]{:S(2)}, u32[]{:S(2)}) collective-permute-start(bf16[256,512]{1,0:T(8,128)(2,1)} %get-tuple-element.82), channel_id=1, source_target_pairs={{0,2},{1,3},{2,0},{3,1},{4,6},{5,7},{6,4},{7,5},{8,10},{9,11},{10,... | collective-permute-start | bytes 786440 | tf_op jit(solution)/shard_map/ppermute | solution.py:20
  603.8 15.0 %collective-permute-start.30 = (bf16[256,512]{1,0:T(8,128)(2,1)}, bf16[256,512]{1,0:T(8,128)(2,1)S(1)}, u32[]{:S(2)}, u32[]{:S(2)}) collective-permute-start(bf16[256,512]{1,0:T(8,128)(2,1)} %get-tuple-element.83), channel_id=1, source_target_pairs={{0,3},{1,2},{2,1},{3,0},{4,7},{5,6},{6,5},{7,4},{8,11},{9,10},{10,... | collective-permute-start | bytes 786440 | tf_op jit(solution)/shard_map/ppermute | solution.py:20
  604.9 15.8 %all-to-all-start.1 = ((bf16[8,32,256]{2,1,0:T(8,128)(2,1)}), bf16[8,32,256]{2,1,0:T(8,128)(2,1)S(1)}, u32[]{:S(2)}, u32[]{:S(2)}) async-start(bf16[8,32,256]{2,1,0:T(8,128)(2,1)} %pad_maximum_fusion.5), calls=%async_computation.1 | async-start | bytes 262144 | tf_op jit(solution)/shard_map/all_to_all | solution.py:319
  620.7 18.2 %all-to-all-start = ((bf16[8,32,768]{2,1,0:T(8,128)(2,1)}), bf16[8,32,768]{2,1,0:T(8,128)(2,1)S(1)}, u32[]{:S(2)}, u32[]{:S(2)}) async-start(bf16[8,32,768]{2,1,0:T(8,128)(2,1)} %pad_maximum_fusion.3), calls=%async_computation | async-start | bytes 786432 | tf_op jit(solution)/shard_map/all_to_all | solution.py:319
  (29 other events, 401.3 us)

commit v2 on v1

--- a/solution.py
+++ b/solution.py
@@ -12,7 +12,6 @@
 
 HBM = pltpu.MemorySpace.HBM
 VMEM = pltpu.MemorySpace.VMEM
-SMEM = pltpu.MemorySpace.SMEM
 
 
 def swap(value, axis, k):
@@ -38,9 +37,7 @@
 
 
 def act_kernel(count, per_tp, keys, hidden, *refs):
-    me_ref, x_ref = refs[:2]
-    pieces = refs[2 : 2 + count]
-    refs = refs[2 + count :]
+    x_ref, pieces, refs = refs[0], refs[1 : 1 + count], refs[1 + count :]
     if hidden:
         gate_ref, out_ref, act_ref, held, acc, load_sem, store_sem = refs
     else:
@@ -53,14 +50,14 @@
         load.start()
     stores = []
     for j in range(count):
-        slot = me_ref[0] ^ keys[j]
+        slot = lax.axis_index("fs") ^ keys[j]
         loads[j].wait()
         store = pltpu.make_async_copy(
             held.at[j], out_ref.at[pl.ds(pl.multiple_of(slot * rows, rows), rows)], store_sem.at[j]
         )
         store.start()
         stores.append(store)
-        which = (slot // per_tp ^ me_ref[1]) * per_tp + slot % per_tp
+        which = (slot // per_tp ^ lax.axis_index("tp")) * per_tp + slot % per_tp
         part = jnp.dot(x_ref[which], held[j], preferred_element_type=jnp.float32)
         if j == 0:
             acc[...] = part
@@ -75,12 +72,12 @@
         store.wait()
 
 
-def activate(me, x, pieces, keys, per_tp, gate=None):
+def activate(x, pieces, keys, per_tp, gate=None):
     count = len(pieces)
     rows, columns = pieces[0].shape
     tokens = x.shape[1]
-    args = [me, x, *pieces]
-    in_specs = [pl.BlockSpec(memory_space=SMEM), pl.BlockSpec(memory_space=VMEM)]
+    args = [x, *pieces]
+    in_specs = [pl.BlockSpec(memory_space=VMEM)]
     in_specs += [pl.BlockSpec(memory_space=HBM)] * count
     if gate is not None:
         args.append(gate)
@@ -103,25 +100,14 @@
     )(*args)
 
 
-def fetch(keys, offsets, rows, width, start, me_ref, pieces, out_ref, held, load_sem, place_sem):
-    loads, places = [], []
-    for j in range(len(keys)):
-        slot = me_ref[0] ^ keys[j]
-        spot = held.at[pl.ds(pl.multiple_of(slot * rows, rows), rows)]
+def down_kernel(keys, offsets, rows, hidden_ref, *refs):
+    pieces, blocks = refs[: len(keys)], refs[len(keys) : -6]
+    hidden, held, sums, hidden_sem, load_sem, store_sem = refs[-6:]
+    loads = []
+    for j, key in enumerate(keys):
+        spot = held.at[pl.ds(pl.multiple_of((lax.axis_index("fs") ^ key) * rows, rows), rows)]
         piece = pieces[j].at[pl.ds(offsets[j], rows)]
         loads.append(pltpu.make_async_copy(piece, spot, load_sem.at[j]))
-        if out_ref is not None:
-            first = pl.multiple_of(slot * width + start, 16)
-            places.append(
-                pltpu.make_async_copy(spot, out_ref.at[pl.ds(first, rows)], place_sem.at[j])
-            )
-    return loads, places
-
-
-def down_kernel(keys, offsets, rows, me_ref, hidden_ref, *refs):
-    pieces, blocks = refs[: len(keys)], refs[len(keys) : -6]
-    hidden, held, sums, hidden_sem, load_sem, store_sem = refs[-6:]
-    loads, _ = fetch(keys, offsets, rows, 0, 0, me_ref, pieces, None, held, load_sem, None)
     loads.append(pltpu.make_async_copy(hidden_ref, hidden, hidden_sem))
     for load in loads:
         load.start()
@@ -130,7 +116,7 @@
     span = held.shape[0] // len(blocks)
     stores = []
     for rel in reversed(range(len(blocks))):
-        block = me_ref[1] ^ rel
+        block = lax.axis_index("tp") ^ rel
         part = lax.dot_general(
             hidden[...],
             held[pl.ds(pl.multiple_of(block * span, span), span)],
@@ -145,15 +131,14 @@
         store.wait()
 
 
-def down_partial(me, hidden, pieces, keys, parts, width, start, rows):
+def down_partial(hidden, pieces, keys, parts, width, start, rows):
     count = len(pieces)
     columns = pieces[0].shape[1]
     offsets = [start if piece.shape[0] == width else 0 for piece in pieces]
     block = jax.ShapeDtypeStruct((hidden.shape[0], count * rows // parts), jnp.bfloat16)
     return pl.pallas_call(
         functools.partial(down_kernel, keys, offsets, rows),
-        in_specs=[pl.BlockSpec(memory_space=SMEM)]
-        + [pl.BlockSpec(memory_space=HBM)] * (1 + count),
+        in_specs=[pl.BlockSpec(memory_space=HBM)] * (1 + count),
         out_specs=[pl.BlockSpec(memory_space=HBM)] * parts,
         out_shape=[block] * parts,
         scratch_shapes=[
@@ -164,15 +149,21 @@
             pltpu.SemaphoreType.DMA((count,)),
             pltpu.SemaphoreType.DMA((parts,)),
         ],
-    )(me, hidden, *pieces)
-
-
-def place_kernel(keys, offsets, rows, width, start, aliased, me_ref, *refs):
-    pieces = refs[: len(keys)]
-    out_ref, held, load_sem, place_sem = refs[len(keys) + aliased :]
-    loads, places = fetch(
-        keys, offsets, rows, width, start, me_ref, pieces, out_ref, held, load_sem, place_sem
-    )
+    )(hidden, *pieces)
+
+
+def place_kernel(moves, width, aliased, *refs):
+    pieces = refs[: len(moves)]
+    out_ref, held, load_sem, place_sem = refs[len(moves) + aliased :]
+    loads, places = [], []
+    place = 0
+    for j, (key, offset, start, rows) in enumerate(moves):
+        spot = held.at[pl.ds(place, rows)]
+        first = pl.multiple_of((lax.axis_index("fs") ^ key) * width + start, 16)
+        piece = pieces[j].at[pl.ds(offset, rows)]
+        loads.append(pltpu.make_async_copy(piece, spot, load_sem.at[j]))
+        places.append(pltpu.make_async_copy(spot, out_ref.at[pl.ds(first, rows)], place_sem.at[j]))
+        place += rows
     for load in loads:
         load.start()
     for load, place in zip(loads, places):
@@ -182,25 +173,26 @@
         place.wait()
 
 
-def place_chunk(me, pieces, keys, width, start, rows, out):
-    count = len(pieces)
-    columns = pieces[0].shape[1]
-    offsets = [start if piece.shape[0] == width else 0 for piece in pieces]
-    args = [me, *pieces]
+def place_chunks(chunks, keys, width, spans, out):
+    args, moves = [], []
+    for pieces, (start, rows) in zip(chunks, spans):
+        for key, piece in zip(keys, pieces):
+            args.append(piece)
+            moves.append((key, start if piece.shape[0] == width else 0, start, rows))
+    columns = args[0].shape[1]
     aliases = {}
     if out is not None:
         aliases = {len(args): 0}
         args.append(out)
     return pl.pallas_call(
-        functools.partial(place_kernel, keys, offsets, rows, width, start, len(aliases)),
-        in_specs=[pl.BlockSpec(memory_space=SMEM)]
-        + [pl.BlockSpec(memory_space=HBM)] * (len(args) - 1),
+        functools.partial(place_kernel, moves, width, len(aliases)),
+        in_specs=[pl.BlockSpec(memory_space=HBM)] * len(args),
         out_specs=pl.BlockSpec(memory_space=HBM),
-        out_shape=jax.ShapeDtypeStruct((count * width, columns), jnp.bfloat16),
+        out_shape=jax.ShapeDtypeStruct((len(keys) * width, columns), jnp.bfloat16),
         scratch_shapes=[
-            pltpu.VMEM((count * rows, columns), jnp.bfloat16),
-            pltpu.SemaphoreType.DMA((count,)),
-            pltpu.SemaphoreType.DMA((count,)),
+            pltpu.VMEM((len(keys) * sum(rows for _, rows in spans), columns), jnp.bfloat16),
+            pltpu.SemaphoreType.DMA((len(moves),)),
+            pltpu.SemaphoreType.DMA((len(moves),)),
         ],
         input_output_aliases=aliases,
     )(*args)
@@ -240,13 +232,12 @@
 def per_device(tokens, routes, route_logits, norm_gain, gate_weight, up_weight, down_weight):
     experts, width, _ = gate_weight.shape
     fs_count, tp_count = lax.axis_size("fs"), lax.axis_size("tp")
-    fs_me, tp_me = lax.axis_index("fs"), lax.axis_index("tp")
+    fs_me = lax.axis_index("fs")
     spread = fs_count // experts
     per_tp = fs_count // tp_count
     columns = gate_weight.shape[2] // spread
     own_rows, model = tokens.shape
     part_width = model // tp_count
-    me = jnp.stack([fs_me, tp_me]).astype(jnp.int32)
     near, far, first_order, order = partner_orders(fs_count, spread)
     keys = [0] + near + far
     cuts = [0, width // 2, width * 3 // 4, width * 7 // 8, width]
@@ -298,16 +289,20 @@
     x = blocks.reshape(tp_count, -1, per_tp, width)
     x = jnp.transpose(x, (0, 2, 1, 3)).reshape(fs_count, -1, width)
 
-    gate_out, gate_act = activate(me, x, gate_pieces, keys, per_tp)
-    up_out, hidden = activate(me, x, up_pieces, keys, per_tp, gate_act)
+    gate_out, gate_act = activate(x, gate_pieces, keys, per_tp)
+    up_out, hidden = activate(x, up_pieces, keys, per_tp, gate_act)
 
     down_out = None
     totals = []
-    for span, pieces in zip(spans, down_pieces):
-        parts = down_partial(me, hidden, pieces, keys, tp_count, width, *span)
-        down_out = place_chunk(me, pieces, keys, width, *span, down_out)
+    for c, (span, pieces) in enumerate(zip(spans, down_pieces)):
+        parts = down_partial(hidden, pieces, keys, tp_count, width, *span)
+        if c < 2 or c == len(spans) - 1:
+            first = min(c, 2)
+            down_out = place_chunks(
+                down_pieces[first : c + 1], keys, width, spans[first : c + 1], down_out
+            )
         total = parts[0].astype(jnp.float32)
-        for k in range(1, tp_count):
+        for k in reversed(range(1, tp_count)):
             total = total + swap(parts[k], "tp", k).astype(jnp.float32)
         totals.append(total.astype(jnp.bfloat16).reshape(fs_count, -1, total.shape[1]))
     combine = jnp.broadcast_to(

time: 641 us -> 638 us (level)
  Pallas kernels: 47 us -> 39.9 us
    pallas_call x4 -> x3, Pallas kernels: 12.8 us -> 8.56 us  [place_chunks(): pl.pallas_call(functools.partial(place_kernel, moves, width, len(aliases)...]
  transfers between devices with their start and end apart: 54 -> 54, of which waited for: 19 -> 20; matrix products, arithmetic and copies ran while one was open for 8% -> 7% of each run, Pallas kernels for 7% -> 6%
where the time goes in v2:
time: 638 us; the launch traced here: 637 us
  waiting for transfers between devices  273 us (43%)
  starting transfers between devices  272 us (43%)
  Pallas kernels  39.9 us (6%)
  other arithmetic  30.4 us (5%)
  local copies, waits for them, and re-layouts  20.4 us (3%)
    ppermute x52, waiting for transfers between devices, swap(): return lax.ppermute(value, axis, [(i, i ^ k) for i in range(count)])  271 us
    ppermute x52, starting transfers between devices, swap(): return lax.ppermute(value, axis, [(i, i ^ k) for i in range(count)])  261 us
    convert_element_type x4, other arithmetic, make_piece(): return piece.astype(jnp.bfloat16)  24 us
    pallas_call x2, Pallas kernels, activate(): pl.pallas_call(functools.partial(act_kernel, count, per_tp, keys, gate is...  18.1 us
    convert_element_type x5, local copies, waits for them, and re-layouts, make_piece(): return piece.astype(jnp.bfloat16)  15.3 us
    pallas_call x4, Pallas kernels, down_partial(): pl.pallas_call(functools.partial(down_kernel, keys, offsets, rows), in_sp...  13.3 us
  transfers between devices with their start and end apart: 54, of which 20 were waited for; matrix products, arithmetic and copies ran while one was open for 7% of the time, Pallas kernels for 6%

profile of v2, /device:TPU:0, one launch (start us, length us, event | category | flops | bytes accessed | tf_op | source)
XLA Modules:
  0.0 637.3 jit_solution(11187511597065465022)
XLA Ops:
  0.7 1.8 fusion.15
  3.3 5.1 collective-permute-start.2
  8.5 8.6 %fusion.9 = (bf16[512,1024]{1,0:T(8,128)(2,1)}, bf16[512,1024]{1,0:T(8,128)(2,1)}, bf16[512,1024]{1,0:T(8,128)(2,1)}, bf16[512,1024]{1,0:T(8,128)(2,1)}, bf16[51...) fusion(f32[4,512,2048]{2,1,0:T(8,128)} %param.13, s32[]{:T(128)S(6)} %select_n.244, s32[]{:T(128)S(6)} %select_n.245, ...), kind=kLoop, calls=%fused_computation.25 | loop fusion | flops 6291456 | bytes 18876464 | tf_op jit(solution)/shard_map/convert_element_type | solution.py:36
  17.1 9.6 %fusion.2 = (bf16[512,1024]{1,0:T(8,128)(2,1)}, bf16[512,1024]{1,0:T(8,128)(2,1)}, bf16[512,1024]{1,0:T(8,128)(2,1)}, bf16[512,1024]{1,0:T(8,128)(2,1)}, bf16[51...) fusion(f32[4,512,2048]{2,1,0:T(8,128)} %param.14, s32[]{:T(128)S(6)} %select_n.244, ...), kind=kLoop, calls=%fused_computation.11 | loop fusion | flops 7340032 | bytes 22022200 | tf_op jit(solution)/shard_map/convert_element_type | solution.py:36
  26.6 1.7 fusion.36
  28.3 2.9 collective-permute-start.47
  31.2 1.9 collective-permute-start.48
  34.2 2.4 fusion.27
  40.1 2.4 collective-permute-done
  42.4 2.2 collective-permute-start.40
  44.6 2.6 collective-permute-start.41
  47.2 9.5 %collective-permute-start.38 = (bf16[64,1024]{1,0:T(8,128)(2,1)S(1)}, bf16[64,1024]{1,0:T(8,128)(2,1)S(1)}, u32[]{:S(2)}, u32[]{:S(2)}) collective-permute-start(bf16[64,1024]{1,0:T(8,128)(2,1)S(1)} %get-tuple-element.120), channel_id=1, source_target_pairs={{0,20},{4,16},{8,28},{12,24},{16,4},{20,0},{24,12},{28,8},{1,21},{... | collective-permute-start | bytes 393224 | tf_op jit(solution)/shard_map/ppermute | solution.py:19
  56.7 3.3 collective-permute-done.45.refs_4_.refs_12_
  61.9 4.6 collective-permute-done.46.refs_5_.refs_13_
  66.5 26.3 %collective-permute-start.14 = (bf16[512,1024]{1,0:T(8,128)(2,1)}, bf16[512,1024]{1,0:T(8,128)(2,1)}, u32[]{:S(2)}, u32[]{:S(2)}) collective-permute-start(bf16[512,1024]{1,0:T(8,128)(2,1)} %get-tuple-element.70), channel_id=1, source_target_pairs={{0,8},{4,12},{8,0},{12,4},{16,24},{20,28},{24,16},{28,20},{1,9},{5... | collective-permute-start | bytes 3145736 | tf_op jit(solution)/shard_map/ppermute | solution.py:19
  92.9 2.7 collective-permute-start.33
  95.6 2.4 collective-permute-done.38.refs_4_
  98.0 1.9 collective-permute-start.34
  101.4 5.9 collective-permute-done.3
  108.1 17.5 %collective-permute-done.33.refs_6_ = bf16[128,1024]{1,0:T(8,128)(2,1)S(1)} collective-permute-done((bf16[128,1024]{1,0:T(8,128)(2,1)}, bf16[128,1024]{1,0:T(8,128)(2,1)S(1)}, u32[]{:S(2)}, u32[]{:S(2)}) %collective-permute-start.33) | collective-permute-done | bytes 262176 | tf_op jit(solution)/shard_map/ppermute | solution.py:19
  125.6 23.5 %collective-permute-done.34.refs_7_ = bf16[128,1024]{1,0:T(8,128)(2,1)S(1)} collective-permute-done((bf16[128,1024]{1,0:T(8,128)(2,1)}, bf16[128,1024]{1,0:T(8,128)(2,1)S(1)}, u32[]{:S(2)}, u32[]{:S(2)}) %collective-permute-start.34) | collective-permute-done | bytes 262176 | tf_op jit(solution)/shard_map/ppermute | solution.py:19
  150.7 5.4 collective-permute-done.31.refs_4_
  156.2 3.0 collective-permute-start.15
  159.1 1.7 collective-permute-done.5
  160.8 9.5 %collective-permute-start.16 = (bf16[512,1024]{1,0:T(8,128)(2,1)}, bf16[512,1024]{1,0:T(8,128)(2,1)}, u32[]{:S(2)}, u32[]{:S(2)}) collective-permute-start(bf16[512,1024]{1,0:T(8,128)(2,1)} %get-tuple-element.72), channel_id=1, source_target_pairs={{0,12},{4,8},{8,4},{12,0},{16,28},{20,24},{24,20},{28,16},{1,13},{... | collective-permute-start | bytes 3145736 | tf_op jit(solution)/shard_map/ppermute | solution.py:19
  170.3 2.8 collective-permute-start.17
  173.2 2.0 collective-permute-start.19
  175.2 1.8 collective-permute-start.20
  177.0 73.4 %collective-permute-done.15.refs_3_ = bf16[512,1024]{1,0:T(8,128)(2,1)} collective-permute-done((bf16[512,1024]{1,0:T(8,128)(2,1)}, bf16[512,1024]{1,0:T(8,128)(2,1)}, u32[]{:S(2)}, u32[]{:S(2)}) %collective-permute-start.15) | collective-permute-done | bytes 1048608 | tf_op jit(solution)/shard_map/ppermute | solution.py:19
  251.7 14.4 %collective-permute-done.17.refs_5_ = bf16[512,1024]{1,0:T(8,128)(2,1)} collective-permute-done((bf16[512,1024]{1,0:T(8,128)(2,1)}, bf16[512,1024]{1,0:T(8,128)(2,1)}, u32[]{:S(2)}, u32[]{:S(2)}) %collective-permute-start.17) | collective-permute-done | bytes 1048608 | tf_op jit(solution)/shard_map/ppermute | solution.py:19
  267.4 25.0 %collective-permute-start.10 = (bf16[512,1024]{1,0:T(8,128)(2,1)}, bf16[512,1024]{1,0:T(8,128)(2,1)S(1)}, u32[]{:S(2)}, u32[]{:S(2)}) collective-permute-start(bf16[512,1024]{1,0:T(8,128)(2,1)} %get-tuple-element.65), channel_id=1, source_target_pairs={{0,20},{4,16},{8,28},{12,24},{16,4},{20,0},{24,12},{28,8},{1,21},{... | collective-permute-start | bytes 3145736 | tf_op jit(solution)/shard_map/ppermute | solution.py:19
  292.3 77.2 %collective-permute-start.11 = (bf16[512,1024]{1,0:T(8,128)(2,1)}, bf16[512,1024]{1,0:T(8,128)(2,1)S(1)}, u32[]{:S(2)}, u32[]{:S(2)}) collective-permute-start(bf16[512,1024]{1,0:T(8,128)(2,1)} %get-tuple-element.66), channel_id=1, source_target_pairs={{0,16},{4,20},{8,24},{12,28},{16,0},{20,4},{24,8},{28,12},{1,17},{... | collective-permute-start | bytes 3145736 | tf_op jit(solution)/shard_map/ppermute | solution.py:19
  369.6 1.6 collective-permute-start.12
  371.2 3.4 collective-permute-start.13
  374.6 4.8 fusion.19
  379.5 44.3 %collective-permute-done.10.refs_5_ = bf16[512,1024]{1,0:T(8,128)(2,1)S(1)} collective-permute-done((bf16[512,1024]{1,0:T(8,128)(2,1)}, bf16[512,1024]{1,0:T(8,128)(2,1)S(1)}, u32[]{:S(2)}, u32[]{:S(2)}) %collective-permute-start.10) | collective-permute-done | bytes 1048608 | tf_op jit(solution)/shard_map/ppermute | solution.py:19
  423.8 2.8 collective-permute-start.22
  426.6 20.9 %collective-permute-done.11.refs_6_ = bf16[512,1024]{1,0:T(8,128)(2,1)S(1)} collective-permute-done((bf16[512,1024]{1,0:T(8,128)(2,1)}, bf16[512,1024]{1,0:T(8,128)(2,1)S(1)}, u32[]{:S(2)}, u32[]{:S(2)}) %collective-permute-start.11) | collective-permute-done | bytes 1048608 | tf_op jit(solution)/shard_map/ppermute | solution.py:19
  448.6 3.7 fusion.23
  452.3 2.7 fusion.16.refs_0_.refs_8_
  455.0 4.0 fusion
  459.0 2.7 collective-permute-start.26
  463.1 54.4 %collective-permute-start.32 = (bf16[128,1024]{1,0:T(8,128)(2,1)}, bf16[128,1024]{1,0:T(8,128)(2,1)S(1)}, u32[]{:S(2)}, u32[]{:S(2)}) collective-permute-start(bf16[128,1024]{1,0:T(8,128)(2,1)} %get-tuple-element.125), channel_id=1, source_target_pairs={{0,16},{4,20},{8,24},{12,28},{16,0},{20,4},{24,8},{28,12},{1,17},{... | collective-permute-start | bytes 786440 | tf_op jit(solution)/shard_map/ppermute | solution.py:19
  517.5 2.6 collective-permute-start.25
  521.8 9.0 %shard_map.120 = (bf16[4096,1024]{1,0:T(8,128)(2,1)}, f32[256,1024]{1,0:T(8,128)}) custom-call(bf16[8,256,512]{2,1,0:T(8,128)(2,1)} %bitcast.157, bf16[512,1024]{1,0:T(8,128)(2,1)} %get-tuple-element.138.refs_1_, bf16[512,1024]{1,0:T(8,128)(2,1)} %collective-permute-done.14.refs_2_, bf16[512,1024]{1,0:T(8,128)(2,1)} %collective-permute-done.15.refs_3_, ...), custom_call_target="tpu_custom_call" | custom-call | tf_op jit(solution)/shard_map/pallas_call | solution.py:86
  530.8 9.1 %shard_map.121 = (bf16[4096,1024]{1,0:T(8,128)(2,1)}, bf16[256,1024]{1,0:T(8,128)(2,1)}) custom-call(bf16[8,256,512]{2,1,0:T(8,128)(2,1)} %bitcast.158, bf16[512,1024]{1,0:T(8,128)(2,1)} %get-tuple-element.139.refs_1_, bf16[512,1024]{1,0:T(8,128)(2,1)} %collective-permute-done.7.refs_2_, bf16[512,1024]{1,0:T(8,128)(2,1)} %collective-permute-done.8.refs_3_, ...), custom_call_target="tpu_custom_call" | custom-call | tf_op jit(solution)/shard_map/pallas_call | solution.py:86
  539.9 2.8 shard_map.125
  542.8 28.4 %collective-permute-done.32.refs_5_ = bf16[128,1024]{1,0:T(8,128)(2,1)S(1)} collective-permute-done((bf16[128,1024]{1,0:T(8,128)(2,1)}, bf16[128,1024]{1,0:T(8,128)(2,1)S(1)}, u32[]{:S(2)}, u32[]{:S(2)}) %collective-permute-start.32) | collective-permute-done | bytes 262176 | tf_op jit(solution)/shard_map/ppermute | solution.py:19
  571.3 1.8 collective-permute-start.51
  573.1 2.8 shard_map.124
  575.9 3.3 shard_map.123
  579.2 2.0 collective-permute-done.24.refs_4_
  581.2 11.5 %collective-permute-done.25.refs_5_ = bf16[256,1024]{1,0:T(8,128)(2,1)} collective-permute-done((bf16[256,1024]{1,0:T(8,128)(2,1)}, bf16[256,1024]{1,0:T(8,128)(2,1)}, u32[]{:S(2)}, u32[]{:S(2)}) %collective-permute-start.25) | collective-permute-done | bytes 524320 | tf_op jit(solution)/shard_map/ppermute | solution.py:19
  593.3 4.4 shard_map.122
  597.9 1.6 collective-permute-start.35
  600.1 1.6 collective-permute-start.28
  604.8 5.1 all-to-all-start.1
  610.0 1.9 collective-permute-done.28
  611.9 5.9 collective-permute-done.29
  619.7 5.1 all-to-all-start
  625.2 3.6 shard_map.126.refs_8_
  628.7 2.4 shard_map.127.refs_16_
  631.1 2.6 shard_map.128
  634.1 2.0 all-to-all-done
  (199 shorter events, 25.8 us)
Async XLA Ops:
  3.3 34.8 %collective-permute-start.2 = (bf16[32,1024]{1,0:T(8,128)(2,1)S(1)}, bf16[32,1024]{1,0:T(8,128)(2,1)S(1)}, u32[]{:S(2)}, u32[]{:S(2)}) collective-permute-start(bf16[32,1024]{1,0:T(8,128)(2,1)S(1)} %get-tuple-element.133), channel_id=1, source_target_pairs={{0,24},{4,28},{8,16},{12,20},{16,8},{20,12},{24,0},{28,4},{1,25},{... | collective-permute-start | bytes 196616 | tf_op jit(solution)/shard_map/ppermute | solution.py:19
  8.5 31.1 %collective-permute-start.1 = (bf16[32,1024]{1,0:T(8,128)(2,1)S(1)}, bf16[32,1024]{1,0:T(8,128)(2,1)S(1)}, u32[]{:S(2)}, u32[]{:S(2)}) collective-permute-start(bf16[32,1024]{1,0:T(8,128)(2,1)S(1)} %get-tuple-element.134), channel_id=1, source_target_pairs={{0,16},{4,20},{8,24},{12,28},{16,0},{20,4},{24,8},{28,12},{1,17},{... | collective-permute-start | bytes 196616 | tf_op jit(solution)/shard_map/ppermute | solution.py:19
  28.3 16.3 %collective-permute-start.47 = (bf16[64,1024]{1,0:T(8,128)(2,1)S(1)}, bf16[64,1024]{1,0:T(8,128)(2,1)S(1)}, u32[]{:S(2)}, u32[]{:S(2)}) collective-permute-start(bf16[64,1024]{1,0:T(8,128)(2,1)S(1)} %get-tuple-element.114), channel_id=1, source_target_pairs={{0,28},{4,24},{8,20},{12,16},{16,12},{20,8},{24,4},{28,0},{1,29},{... | collective-permute-start | bytes 393224 | tf_op jit(solution)/shard_map/ppermute | solution.py:19
  31.2 16.0 %collective-permute-start.48 = (bf16[64,1024]{1,0:T(8,128)(2,1)S(1)}, bf16[64,1024]{1,0:T(8,128)(2,1)S(1)}, u32[]{:S(2)}, u32[]{:S(2)}) collective-permute-start(bf16[64,1024]{1,0:T(8,128)(2,1)S(1)} %get-tuple-element.115), channel_id=1, source_target_pairs={{0,24},{4,28},{8,16},{12,20},{16,8},{20,12},{24,0},{28,4},{1,25},{... | collective-permute-start | bytes 393224 | tf_op jit(solution)/shard_map/ppermute | solution.py:19
  33.1 26.9 %collective-permute-start.45 = (bf16[64,1024]{1,0:T(8,128)(2,1)S(1)}, bf16[64,1024]{1,0:T(8,128)(2,1)S(1)}, u32[]{:S(2)}, u32[]{:S(2)}) collective-permute-start(bf16[64,1024]{1,0:T(8,128)(2,1)S(1)} %get-tuple-element.116), channel_id=1, source_target_pairs={{0,20},{4,16},{8,28},{12,24},{16,4},{20,0},{24,12},{28,8},{1,21},{... | collective-permute-start | bytes 393224 | tf_op jit(solution)/shard_map/ppermute | solution.py:19
  38.1 4.3 collective-permute-start
  39.5 27.0 %collective-permute-start.46 = (bf16[64,1024]{1,0:T(8,128)(2,1)S(1)}, bf16[64,1024]{1,0:T(8,128)(2,1)S(1)}, u32[]{:S(2)}, u32[]{:S(2)}) collective-permute-start(bf16[64,1024]{1,0:T(8,128)(2,1)S(1)} %get-tuple-element.117), channel_id=1, source_target_pairs={{0,16},{4,20},{8,24},{12,28},{16,0},{20,4},{24,8},{28,12},{1,17},{... | collective-permute-start | bytes 393224 | tf_op jit(solution)/shard_map/ppermute | solution.py:19
  42.4 24.1 %collective-permute-start.40 = (bf16[64,1024]{1,0:T(8,128)(2,1)S(1)}, bf16[64,1024]{1,0:T(8,128)(2,1)S(1)}, u32[]{:S(2)}, u32[]{:S(2)}) collective-permute-start(bf16[64,1024]{1,0:T(8,128)(2,1)S(1)} %get-tuple-element.118), channel_id=1, source_target_pairs={{0,28},{4,24},{8,20},{12,16},{16,12},{20,8},{24,4},{28,0},{1,29},{... | collective-permute-start | bytes 393224 | tf_op jit(solution)/shard_map/ppermute | solution.py:19
  44.6 63.4 %copy-start.14 = (bf16[64,1024]{1,0:T(8,128)(2,1)}, bf16[64,1024]{1,0:T(8,128)(2,1)S(1)}, u32[]{:S(2)}) copy-start(bf16[64,1024]{1,0:T(8,128)(2,1)S(1)} %collective-permute-done.47.refs_6_.refs_14_) | copy-start | bytes 393220
  44.6 48.3 %collective-permute-start.41 = (bf16[64,1024]{1,0:T(8,128)(2,1)S(1)}, bf16[64,1024]{1,0:T(8,128)(2,1)S(1)}, u32[]{:S(2)}, u32[]{:S(2)}) collective-permute-start(bf16[64,1024]{1,0:T(8,128)(2,1)S(1)} %get-tuple-element.119), channel_id=1, source_target_pairs={{0,24},{4,28},{8,16},{12,20},{16,8},{20,12},{24,0},{28,4},{1,25},{... | collective-permute-start | bytes 393224 | tf_op jit(solution)/shard_map/ppermute | solution.py:19
  47.2 50.8 %collective-permute-start.38 = (bf16[64,1024]{1,0:T(8,128)(2,1)S(1)}, bf16[64,1024]{1,0:T(8,128)(2,1)S(1)}, u32[]{:S(2)}, u32[]{:S(2)}) collective-permute-start(bf16[64,1024]{1,0:T(8,128)(2,1)S(1)} %get-tuple-element.120), channel_id=1, source_target_pairs={{0,20},{4,16},{8,28},{12,24},{16,4},{20,0},{24,12},{28,8},{1,21},{... | collective-permute-start | bytes 393224 | tf_op jit(solution)/shard_map/ppermute | solution.py:19
  60.0 39.9 %collective-permute-start.39 = (bf16[64,1024]{1,0:T(8,128)(2,1)S(1)}, bf16[64,1024]{1,0:T(8,128)(2,1)S(1)}, u32[]{:S(2)}, u32[]{:S(2)}) collective-permute-start(bf16[64,1024]{1,0:T(8,128)(2,1)S(1)} %get-tuple-element.121), channel_id=1, source_target_pairs={{0,16},{4,20},{8,24},{12,28},{16,0},{20,4},{24,8},{28,12},{1,17},{... | collective-permute-start | bytes 393224 | tf_op jit(solution)/shard_map/ppermute | solution.py:19
  66.5 106.6 %collective-permute-start.18 = (bf16[512,1024]{1,0:T(8,128)(2,1)S(1)}, bf16[512,1024]{1,0:T(8,128)(2,1)}, u32[]{:S(2)}, u32[]{:S(2)}) collective-permute-start(bf16[512,1024]{1,0:T(8,128)(2,1)S(1)} %fusion.15), channel_id=1, source_target_pairs={{0,16},{4,20},{8,24},{12,28},{16,0},{20,4},{24,8},{28,12},{1,17},{... | collective-permute-start | bytes 3145736 | tf_op jit(solution)/shard_map/ppermute | solution.py:19
  66.5 108.7 %collective-permute-start.14 = (bf16[512,1024]{1,0:T(8,128)(2,1)}, bf16[512,1024]{1,0:T(8,128)(2,1)}, u32[]{:S(2)}, u32[]{:S(2)}) collective-permute-start(bf16[512,1024]{1,0:T(8,128)(2,1)} %get-tuple-element.70), channel_id=1, source_target_pairs={{0,8},{4,12},{8,0},{12,4},{16,24},{20,28},{24,16},{28,20},{1,9},{5... | collective-permute-start | bytes 3145736 | tf_op jit(solution)/shard_map/ppermute | solution.py:19
  92.9 32.7 %collective-permute-start.33 = (bf16[128,1024]{1,0:T(8,128)(2,1)}, bf16[128,1024]{1,0:T(8,128)(2,1)S(1)}, u32[]{:S(2)}, u32[]{:S(2)}) collective-permute-start(bf16[128,1024]{1,0:T(8,128)(2,1)} %get-tuple-element.122), channel_id=1, source_target_pairs={{0,28},{4,24},{8,20},{12,16},{16,12},{20,8},{24,4},{28,0},{1,29},{... | collective-permute-start | bytes 786440 | tf_op jit(solution)/shard_map/ppermute | solution.py:19
  98.0 51.1 %collective-permute-start.34 = (bf16[128,1024]{1,0:T(8,128)(2,1)}, bf16[128,1024]{1,0:T(8,128)(2,1)S(1)}, u32[]{:S(2)}, u32[]{:S(2)}) collective-permute-start(bf16[128,1024]{1,0:T(8,128)(2,1)} %get-tuple-element.123), channel_id=1, source_target_pairs={{0,24},{4,28},{8,16},{12,20},{16,8},{20,12},{24,0},{28,4},{1,25},{... | collective-permute-start | bytes 786440 | tf_op jit(solution)/shard_map/ppermute | solution.py:19
  99.9 7.4 %collective-permute-start.3 = (bf16[4,32,1024]{2,1,0:T(8,128)(2,1)S(1)}, bf16[4,32,1024]{2,1,0:T(8,128)(2,1)S(1)}, u32[]{:S(2)}, u32[]{:S(2)}) collective-permute-start(bf16[4,32,1024]{2,1,0:T(8,128)(2,1)S(1)} %gather_fusion.1), channel_id=1, source_target_pairs={{0,4},{4,0},{8,12},{12,8},{16,20},{20,16},{24,28},{28,24},{1,5},{5... | collective-permute-start | bytes 786440 | tf_op jit(solution)/shard_map/ppermute | solution.py:19
  107.3 48.8 %collective-permute-start.31 = (bf16[128,1024]{1,0:T(8,128)(2,1)S(1)}, bf16[128,1024]{1,0:T(8,128)(2,1)S(1)}, u32[]{:S(2)}, u32[]{:S(2)}) collective-permute-start(bf16[128,1024]{1,0:T(8,128)(2,1)S(1)} %get-tuple-element.124), channel_id=1, source_target_pairs={{0,20},{4,16},{8,28},{12,24},{16,4},{20,0},{24,12},{28,8},{1,21},{... | collective-permute-start | bytes 786440 | tf_op jit(solution)/shard_map/ppermute | solution.py:19
  125.6 253.8 %copy-start.6 = (bf16[128,1024]{1,0:T(8,128)(2,1)}, bf16[128,1024]{1,0:T(8,128)(2,1)S(1)}, u32[]{:S(2)}) copy-start(bf16[128,1024]{1,0:T(8,128)(2,1)S(1)} %collective-permute-done.33.refs_6_) | copy-start | bytes 786436
  125.6 322.9 %copy-start.32 = (f32[40,2]{0,1:T(2,128)S(1)}, f32[40,2]{0,1:T(2,128)}, u32[]{:S(2)}) copy-start(f32[40,2]{0,1:T(2,128)} %param.11) | copy-start | bytes 964
  125.6 30.5 %collective-permute-start.6 = (bf16[256,1024]{1,0:T(8,128)(2,1)S(1)}, bf16[256,1024]{1,0:T(8,128)(2,1)S(1)}, u32[]{:S(2)}, u32[]{:S(2)}) collective-permute-start(bf16[256,1024]{1,0:T(8,128)(2,1)S(1)} %bitcast.160), channel_id=1, source_target_pairs={{0,3},{1,2},{2,1},{3,0},{4,7},{5,6},{6,5},{7,4},{8,11},{9,10},{10,... | collective-permute-start | bytes 1572872 | tf_op jit(solution)/shard_map/ppermute | solution.py:19
  149.2 230.2 %copy-start.7 = (bf16[128,1024]{1,0:T(8,128)(2,1)}, bf16[128,1024]{1,0:T(8,128)(2,1)S(1)}, u32[]{:S(2)}) copy-start(bf16[128,1024]{1,0:T(8,128)(2,1)S(1)} %collective-permute-done.34.refs_7_) | copy-start | bytes 786436
  149.2 11.7 %collective-permute-start.5 = (bf16[256,1024]{1,0:T(8,128)(2,1)S(1)}, bf16[256,1024]{1,0:T(8,128)(2,1)S(1)}, u32[]{:S(2)}, u32[]{:S(2)}) collective-permute-start(bf16[256,1024]{1,0:T(8,128)(2,1)S(1)} %bitcast.161), channel_id=1, source_target_pairs={{0,2},{1,3},{2,0},{3,1},{4,6},{5,7},{6,4},{7,5},{8,10},{9,11},{10,... | collective-permute-start | bytes 1572872 | tf_op jit(solution)/shard_map/ppermute | solution.py:19
  156.1 223.2 %copy-start.8 = (bf16[128,1024]{1,0:T(8,128)(2,1)}, bf16[128,1024]{1,0:T(8,128)(2,1)S(1)}, u32[]{:S(2)}) copy-start(bf16[128,1024]{1,0:T(8,128)(2,1)S(1)} %collective-permute-done.31.refs_4_) | copy-start | bytes 786436
  156.1 14.2 %collective-permute-start.4 = (bf16[256,1024]{1,0:T(8,128)(2,1)S(1)}, bf16[256,1024]{1,0:T(8,128)(2,1)S(1)}, u32[]{:S(2)}, u32[]{:S(2)}) collective-permute-start(bf16[256,1024]{1,0:T(8,128)(2,1)S(1)} %bitcast.162), channel_id=1, source_target_pairs={{0,1},{1,0},{2,3},{3,2},{4,5},{5,4},{6,7},{7,6},{8,9},{9,8},{10,11... | collective-permute-start | bytes 1572872 | tf_op jit(solution)/shard_map/ppermute | solution.py:19
  156.2 136.2 %copy-start.22 = (bf16[256,1024]{1,0:T(8,128)(2,1)}, bf16[256,1024]{1,0:T(8,128)(2,1)S(1)}, u32[]{:S(2)}) copy-start(bf16[256,1024]{1,0:T(8,128)(2,1)S(1)} %collective-permute-done.6) | copy-start | bytes 1572868
  156.2 94.2 %collective-permute-start.15 = (bf16[512,1024]{1,0:T(8,128)(2,1)}, bf16[512,1024]{1,0:T(8,128)(2,1)}, u32[]{:S(2)}, u32[]{:S(2)}) collective-permute-start(bf16[512,1024]{1,0:T(8,128)(2,1)} %get-tuple-element.71), channel_id=1, source_target_pairs={{0,4},{4,0},{8,12},{12,8},{16,20},{20,16},{24,28},{28,24},{1,5},{5... | collective-permute-start | bytes 3145736 | tf_op jit(solution)/shard_map/ppermute | solution.py:19
  160.8 131.5 %copy-start.24 = (bf16[256,1024]{1,0:T(8,128)(2,1)}, bf16[256,1024]{1,0:T(8,128)(2,1)S(1)}, u32[]{:S(2)}) copy-start(bf16[256,1024]{1,0:T(8,128)(2,1)S(1)} %collective-permute-done.5) | copy-start | bytes 1572868
  160.8 89.6 %collective-permute-start.16 = (bf16[512,1024]{1,0:T(8,128)(2,1)}, bf16[512,1024]{1,0:T(8,128)(2,1)}, u32[]{:S(2)}, u32[]{:S(2)}) collective-permute-start(bf16[512,1024]{1,0:T(8,128)(2,1)} %get-tuple-element.72), channel_id=1, source_target_pairs={{0,12},{4,8},{8,4},{12,0},{16,28},{20,24},{24,20},{28,16},{1,13},{... | collective-permute-start | bytes 3145736 | tf_op jit(solution)/shard_map/ppermute | solution.py:19
  170.3 199.2 %copy-start.26 = (bf16[256,1024]{1,0:T(8,128)(2,1)}, bf16[256,1024]{1,0:T(8,128)(2,1)S(1)}, u32[]{:S(2)}) copy-start(bf16[256,1024]{1,0:T(8,128)(2,1)S(1)} %collective-permute-done.4) | copy-start | bytes 1572868
  170.3 95.7 %collective-permute-start.17 = (bf16[512,1024]{1,0:T(8,128)(2,1)}, bf16[512,1024]{1,0:T(8,128)(2,1)}, u32[]{:S(2)}, u32[]{:S(2)}) collective-permute-start(bf16[512,1024]{1,0:T(8,128)(2,1)} %get-tuple-element.73), channel_id=1, source_target_pairs={{0,20},{4,16},{8,28},{12,24},{16,4},{20,0},{24,12},{28,8},{1,21},{... | collective-permute-start | bytes 3145736 | tf_op jit(solution)/shard_map/ppermute | solution.py:19
  173.2 94.2 %collective-permute-start.19 = (bf16[512,1024]{1,0:T(8,128)(2,1)}, bf16[512,1024]{1,0:T(8,128)(2,1)S(1)}, u32[]{:S(2)}, u32[]{:S(2)}) collective-permute-start(bf16[512,1024]{1,0:T(8,128)(2,1)} %get-tuple-element.75), channel_id=1, source_target_pairs={{0,28},{4,24},{8,20},{12,16},{16,12},{20,8},{24,4},{28,0},{1,29},{... | collective-permute-start | bytes 3145736 | tf_op jit(solution)/shard_map/ppermute | solution.py:19
  175.2 117.1 %collective-permute-start.20 = (bf16[512,1024]{1,0:T(8,128)(2,1)}, bf16[512,1024]{1,0:T(8,128)(2,1)}, u32[]{:S(2)}, u32[]{:S(2)}) collective-permute-start(bf16[512,1024]{1,0:T(8,128)(2,1)} %get-tuple-element.76), channel_id=1, source_target_pairs={{0,24},{4,28},{8,16},{12,20},{16,8},{20,12},{24,0},{28,4},{1,25},{... | collective-permute-start | bytes 3145736 | tf_op jit(solution)/shard_map/ppermute | solution.py:19
  250.4 119.2 %collective-permute-start.7 = (bf16[512,1024]{1,0:T(8,128)(2,1)}, bf16[512,1024]{1,0:T(8,128)(2,1)}, u32[]{:S(2)}, u32[]{:S(2)}) collective-permute-start(bf16[512,1024]{1,0:T(8,128)(2,1)} %get-tuple-element.62), channel_id=1, source_target_pairs={{0,8},{4,12},{8,0},{12,4},{16,24},{20,28},{24,16},{28,20},{1,9},{5... | collective-permute-start | bytes 3145736 | tf_op jit(solution)/shard_map/ppermute | solution.py:19
  250.4 120.8 %collective-permute-start.8 = (bf16[512,1024]{1,0:T(8,128)(2,1)}, bf16[512,1024]{1,0:T(8,128)(2,1)}, u32[]{:S(2)}, u32[]{:S(2)}) collective-permute-start(bf16[512,1024]{1,0:T(8,128)(2,1)} %get-tuple-element.63), channel_id=1, source_target_pairs={{0,4},{4,0},{8,12},{12,8},{16,20},{20,16},{24,28},{28,24},{1,5},{5... | collective-permute-start | bytes 3145736 | tf_op jit(solution)/shard_map/ppermute | solution.py:19
  266.0 113.3 %collective-permute-start.9 = (bf16[512,1024]{1,0:T(8,128)(2,1)}, bf16[512,1024]{1,0:T(8,128)(2,1)S(1)}, u32[]{:S(2)}, u32[]{:S(2)}) collective-permute-start(bf16[512,1024]{1,0:T(8,128)(2,1)} %get-tuple-element.64), channel_id=1, source_target_pairs={{0,12},{4,8},{8,4},{12,0},{16,28},{20,24},{24,20},{28,16},{1,13},{... | collective-permute-start | bytes 3145736 | tf_op jit(solution)/shard_map/ppermute | solution.py:19
  267.4 112.0 %copy-start.10 = (bf16[512,1024]{1,0:T(8,128)(2,1)}, bf16[512,1024]{1,0:T(8,128)(2,1)S(1)}, u32[]{:S(2)}) copy-start(bf16[512,1024]{1,0:T(8,128)(2,1)S(1)} %collective-permute-done.19.refs_7_) | copy-start | bytes 3145732
  267.4 156.4 %collective-permute-start.10 = (bf16[512,1024]{1,0:T(8,128)(2,1)}, bf16[512,1024]{1,0:T(8,128)(2,1)S(1)}, u32[]{:S(2)}, u32[]{:S(2)}) collective-permute-start(bf16[512,1024]{1,0:T(8,128)(2,1)} %get-tuple-element.65), channel_id=1, source_target_pairs={{0,20},{4,16},{8,28},{12,24},{16,4},{20,0},{24,12},{28,8},{1,21},{... | collective-permute-start | bytes 3145736 | tf_op jit(solution)/shard_map/ppermute | solution.py:19
  292.3 155.2 %collective-permute-start.11 = (bf16[512,1024]{1,0:T(8,128)(2,1)}, bf16[512,1024]{1,0:T(8,128)(2,1)S(1)}, u32[]{:S(2)}, u32[]{:S(2)}) collective-permute-start(bf16[512,1024]{1,0:T(8,128)(2,1)} %get-tuple-element.66), channel_id=1, source_target_pairs={{0,16},{4,20},{8,24},{12,28},{16,0},{20,4},{24,8},{28,12},{1,17},{... | collective-permute-start | bytes 3145736 | tf_op jit(solution)/shard_map/ppermute | solution.py:19
  369.6 89.5 %collective-permute-start.12 = (bf16[512,1024]{1,0:T(8,128)(2,1)}, bf16[512,1024]{1,0:T(8,128)(2,1)}, u32[]{:S(2)}, u32[]{:S(2)}) collective-permute-start(bf16[512,1024]{1,0:T(8,128)(2,1)} %get-tuple-element.67), channel_id=1, source_target_pairs={{0,28},{4,24},{8,20},{12,16},{16,12},{20,8},{24,4},{28,0},{1,29},{... | collective-permute-start | bytes 3145736 | tf_op jit(solution)/shard_map/ppermute | solution.py:19
  371.2 90.5 %collective-permute-start.13 = (bf16[512,1024]{1,0:T(8,128)(2,1)}, bf16[512,1024]{1,0:T(8,128)(2,1)}, u32[]{:S(2)}, u32[]{:S(2)}) collective-permute-start(bf16[512,1024]{1,0:T(8,128)(2,1)} %get-tuple-element.68), channel_id=1, source_target_pairs={{0,24},{4,28},{8,16},{12,20},{16,8},{20,12},{24,0},{28,4},{1,25},{... | collective-permute-start | bytes 3145736 | tf_op jit(solution)/shard_map/ppermute | solution.py:19
  379.4 68.2 %copy-start.11 = (bf16[512,1024]{1,0:T(8,128)(2,1)}, bf16[512,1024]{1,0:T(8,128)(2,1)S(1)}, u32[]{:S(2)}) copy-start(bf16[512,1024]{1,0:T(8,128)(2,1)S(1)} %collective-permute-done.9.refs_4_) | copy-start | bytes 3145732
  379.4 83.7 %collective-permute-start.23 = (bf16[512,1024]{1,0:T(8,128)(2,1)}, bf16[512,1024]{1,0:T(8,128)(2,1)S(1)}, u32[]{:S(2)}, u32[]{:S(2)}) collective-permute-start(bf16[512,1024]{1,0:T(8,128)(2,1)} %get-tuple-element.111), channel_id=1, source_target_pairs={{0,12},{4,8},{8,4},{12,0},{16,28},{20,24},{24,20},{28,16},{1,13},{... | collective-permute-start | bytes 3145736 | tf_op jit(solution)/shard_map/ppermute | solution.py:19
  423.8 93.7 %collective-permute-start.22 = (bf16[512,1024]{1,0:T(8,128)(2,1)}, bf16[512,1024]{1,0:T(8,128)(2,1)S(1)}, u32[]{:S(2)}, u32[]{:S(2)}) collective-permute-start(bf16[512,1024]{1,0:T(8,128)(2,1)} %get-tuple-element.112), channel_id=1, source_target_pairs={{0,4},{4,0},{8,12},{12,8},{16,20},{20,16},{24,28},{28,24},{1,5},{5... | collective-permute-start | bytes 3145736 | tf_op jit(solution)/shard_map/ppermute | solution.py:19
  448.5 69.0 %collective-permute-start.21 = (bf16[512,1024]{1,0:T(8,128)(2,1)}, bf16[512,1024]{1,0:T(8,128)(2,1)S(1)}, u32[]{:S(2)}, u32[]{:S(2)}) collective-permute-start(bf16[512,1024]{1,0:T(8,128)(2,1)} %get-tuple-element.113), channel_id=1, source_target_pairs={{0,8},{4,12},{8,0},{12,4},{16,24},{20,28},{24,16},{28,20},{1,9},{5... | collective-permute-start | bytes 3145736 | tf_op jit(solution)/shard_map/ppermute | solution.py:19
  459.0 112.2 %collective-permute-start.26 = (bf16[256,1024]{1,0:T(8,128)(2,1)}, bf16[256,1024]{1,0:T(8,128)(2,1)}, u32[]{:S(2)}, u32[]{:S(2)}) collective-permute-start(bf16[256,1024]{1,0:T(8,128)(2,1)} %get-tuple-element.126), channel_id=1, source_target_pairs={{0,28},{4,24},{8,20},{12,16},{16,12},{20,8},{24,4},{28,0},{1,29},{... | collective-permute-start | bytes 1572872 | tf_op jit(solution)/shard_map/ppermute | solution.py:19
  461.7 109.6 %collective-permute-start.27 = (bf16[256,1024]{1,0:T(8,128)(2,1)}, bf16[256,1024]{1,0:T(8,128)(2,1)}, u32[]{:S(2)}, u32[]{:S(2)}) collective-permute-start(bf16[256,1024]{1,0:T(8,128)(2,1)} %get-tuple-element.127), channel_id=1, source_target_pairs={{0,24},{4,28},{8,16},{12,20},{16,8},{20,12},{24,0},{28,4},{1,25},{... | collective-permute-start | bytes 1572872 | tf_op jit(solution)/shard_map/ppermute | solution.py:19
  463.1 108.0 %collective-permute-start.32 = (bf16[128,1024]{1,0:T(8,128)(2,1)}, bf16[128,1024]{1,0:T(8,128)(2,1)S(1)}, u32[]{:S(2)}, u32[]{:S(2)}) collective-permute-start(bf16[128,1024]{1,0:T(8,128)(2,1)} %get-tuple-element.125), channel_id=1, source_target_pairs={{0,16},{4,20},{8,24},{12,28},{16,0},{20,4},{24,8},{28,12},{1,17},{... | collective-permute-start | bytes 786440 | tf_op jit(solution)/shard_map/ppermute | solution.py:19
  517.5 63.7 %collective-permute-start.24 = (bf16[256,1024]{1,0:T(8,128)(2,1)}, bf16[256,1024]{1,0:T(8,128)(2,1)}, u32[]{:S(2)}, u32[]{:S(2)}) collective-permute-start(bf16[256,1024]{1,0:T(8,128)(2,1)} %get-tuple-element.128), channel_id=1, source_target_pairs={{0,20},{4,16},{8,28},{12,24},{16,4},{20,0},{24,12},{28,8},{1,21},{... | collective-permute-start | bytes 1572872 | tf_op jit(solution)/shard_map/ppermute | solution.py:19
  517.5 75.2 %collective-permute-start.25 = (bf16[256,1024]{1,0:T(8,128)(2,1)}, bf16[256,1024]{1,0:T(8,128)(2,1)}, u32[]{:S(2)}, u32[]{:S(2)}) collective-permute-start(bf16[256,1024]{1,0:T(8,128)(2,1)} %get-tuple-element.129), channel_id=1, source_target_pairs={{0,16},{4,20},{8,24},{12,28},{16,0},{20,4},{24,8},{28,12},{1,17},{... | collective-permute-start | bytes 1572872 | tf_op jit(solution)/shard_map/ppermute | solution.py:19
  571.2 26.6 %collective-permute-start.49 = (bf16[256,128]{1,0:T(8,128)(2,1)}, bf16[256,128]{1,0:T(8,128)(2,1)S(1)}, u32[]{:S(2)}, u32[]{:S(2)}) collective-permute-start(bf16[256,128]{1,0:T(8,128)(2,1)} %get-tuple-element.93), channel_id=1, source_target_pairs={{0,3},{1,2},{2,1},{3,0},{4,7},{5,6},{6,5},{7,4},{8,11},{9,10},{10,... | collective-permute-start | bytes 196616 | tf_op jit(solution)/shard_map/ppermute | solution.py:19
  571.2 26.7 %collective-permute-start.50 = (bf16[256,128]{1,0:T(8,128)(2,1)}, bf16[256,128]{1,0:T(8,128)(2,1)S(1)}, u32[]{:S(2)}, u32[]{:S(2)}) collective-permute-start(bf16[256,128]{1,0:T(8,128)(2,1)} %get-tuple-element.94), channel_id=1, source_target_pairs={{0,2},{1,3},{2,0},{3,1},{4,6},{5,7},{6,4},{7,5},{8,10},{9,11},{10,... | collective-permute-start | bytes 196616 | tf_op jit(solution)/shard_map/ppermute | solution.py:19
  571.3 28.2 %collective-permute-start.51 = (bf16[256,128]{1,0:T(8,128)(2,1)}, bf16[256,128]{1,0:T(8,128)(2,1)S(1)}, u32[]{:S(2)}, u32[]{:S(2)}) collective-permute-start(bf16[256,128]{1,0:T(8,128)(2,1)} %get-tuple-element.95), channel_id=1, source_target_pairs={{0,1},{1,0},{2,3},{3,2},{4,5},{5,4},{6,7},{7,6},{8,9},{9,8},{10,11... | collective-permute-start | bytes 196616 | tf_op jit(solution)/shard_map/ppermute | solution.py:19
  581.2 18.8 %collective-permute-start.42 = (bf16[256,128]{1,0:T(8,128)(2,1)S(1)}, bf16[256,128]{1,0:T(8,128)(2,1)S(1)}, u32[]{:S(2)}, u32[]{:S(2)}) collective-permute-start(bf16[256,128]{1,0:T(8,128)(2,1)S(1)} %copy-done.40), channel_id=1, source_target_pairs={{0,3},{1,2},{2,1},{3,0},{4,7},{5,6},{6,5},{7,4},{8,11},{9,10},{10,... | collective-permute-start | bytes 196616 | tf_op jit(solution)/shard_map/ppermute | solution.py:19
  592.8 7.4 %collective-permute-start.43 = (bf16[256,128]{1,0:T(8,128)(2,1)S(1)}, bf16[256,128]{1,0:T(8,128)(2,1)S(1)}, u32[]{:S(2)}, u32[]{:S(2)}) collective-permute-start(bf16[256,128]{1,0:T(8,128)(2,1)S(1)} %copy-done.39), channel_id=1, source_target_pairs={{0,2},{1,3},{2,0},{3,1},{4,6},{5,7},{6,4},{7,5},{8,10},{9,11},{10,... | collective-permute-start | bytes 196616 | tf_op jit(solution)/shard_map/ppermute | solution.py:19
  597.8 4.0 collective-permute-start.44
  597.9 5.5 collective-permute-start.35
  599.5 10.4 %collective-permute-start.36 = (bf16[256,256]{1,0:T(8,128)(2,1)S(1)}, bf16[256,256]{1,0:T(8,128)(2,1)S(1)}, u32[]{:S(2)}, u32[]{:S(2)}) collective-permute-start(bf16[256,256]{1,0:T(8,128)(2,1)S(1)} %copy-done.36), channel_id=1, source_target_pairs={{0,2},{1,3},{2,0},{3,1},{4,6},{5,7},{6,4},{7,5},{8,10},{9,11},{10,... | collective-permute-start | bytes 393224 | tf_op jit(solution)/shard_map/ppermute | solution.py:19
  600.0 9.9 %collective-permute-start.37 = (bf16[256,256]{1,0:T(8,128)(2,1)S(1)}, bf16[256,256]{1,0:T(8,128)(2,1)S(1)}, u32[]{:S(2)}, u32[]{:S(2)}) collective-permute-start(bf16[256,256]{1,0:T(8,128)(2,1)S(1)} %copy-done.35), channel_id=1, source_target_pairs={{0,1},{1,0},{2,3},{3,2},{4,5},{5,4},{6,7},{7,6},{8,9},{9,8},{10,11... | collective-permute-start | bytes 393224 | tf_op jit(solution)/shard_map/ppermute | solution.py:19
  600.1 11.7 %collective-permute-start.28 = (bf16[256,512]{1,0:T(8,128)(2,1)}, bf16[256,512]{1,0:T(8,128)(2,1)S(1)}, u32[]{:S(2)}, u32[]{:S(2)}) collective-permute-start(bf16[256,512]{1,0:T(8,128)(2,1)} %get-tuple-element.81), channel_id=1, source_target_pairs={{0,3},{1,2},{2,1},{3,0},{4,7},{5,6},{6,5},{7,4},{8,11},{9,10},{10,... | collective-permute-start | bytes 786440 | tf_op jit(solution)/shard_map/ppermute | solution.py:19
  601.8 16.0 %collective-permute-start.29 = (bf16[256,512]{1,0:T(8,128)(2,1)}, bf16[256,512]{1,0:T(8,128)(2,1)S(1)}, u32[]{:S(2)}, u32[]{:S(2)}) collective-permute-start(bf16[256,512]{1,0:T(8,128)(2,1)} %get-tuple-element.82), channel_id=1, source_target_pairs={{0,2},{1,3},{2,0},{3,1},{4,6},{5,7},{6,4},{7,5},{8,10},{9,11},{10,... | collective-permute-start | bytes 786440 | tf_op jit(solution)/shard_map/ppermute | solution.py:19
  603.4 14.4 %collective-permute-start.30 = (bf16[256,512]{1,0:T(8,128)(2,1)}, bf16[256,512]{1,0:T(8,128)(2,1)S(1)}, u32[]{:S(2)}, u32[]{:S(2)}) collective-permute-start(bf16[256,512]{1,0:T(8,128)(2,1)} %get-tuple-element.83), channel_id=1, source_target_pairs={{0,1},{1,0},{2,3},{3,2},{4,5},{5,4},{6,7},{7,6},{8,9},{9,8},{10,11... | collective-permute-start | bytes 786440 | tf_op jit(solution)/shard_map/ppermute | solution.py:19
  604.8 14.9 %all-to-all-start.1 = ((bf16[8,32,256]{2,1,0:T(8,128)(2,1)}), bf16[8,32,256]{2,1,0:T(8,128)(2,1)S(1)}, u32[]{:S(2)}, u32[]{:S(2)}) async-start(bf16[8,32,256]{2,1,0:T(8,128)(2,1)} %pad_maximum_fusion.5), calls=%async_computation.1 | async-start | bytes 262144 | tf_op jit(solution)/shard_map/all_to_all | solution.py:314
  619.7 16.5 %all-to-all-start = ((bf16[8,32,768]{2,1,0:T(8,128)(2,1)}), bf16[8,32,768]{2,1,0:T(8,128)(2,1)S(1)}, u32[]{:S(2)}, u32[]{:S(2)}) async-start(bf16[8,32,768]{2,1,0:T(8,128)(2,1)} %pad_maximum_fusion.3), calls=%async_computation | async-start | bytes 786432 | tf_op jit(solution)/shard_map/all_to_all | solution.py:314
  (31 other events, 395.8 us)
